TPU v7x, 512 devices: a whole 4x4x16 slice. The times are simulated.
512 devices in a mesh: dp: 4 (over x), kv: 64 (over z, y), tp: 2 (over core).
Axes of the slice: x: 4, y: 4, z: 16, core: 2. Of those that a mesh axis runs over, the one named last changes fastest.
Arguments:
- tokens: bfloat16 [512, 4096], P('dp', 'kv'), parts along dimension 0, may hold values from -16 to 16
- gain_mix: float32 [4096], P('kv'), may hold values from 0.1 to 1.9
- w_query: bfloat16 [4096, 2048], P('kv', 'tp'), may hold values from -0.09375 to 0.09375
- w_key: bfloat16 [4096, 2048], P('kv', 'tp'), may hold values from -0.09375 to 0.09375
- w_value: bfloat16 [4096, 2048], P('kv', 'tp'), may hold values from -0.09375 to 0.09375
- w_igate: bfloat16 [4096, 16], P('kv', 'tp'), may hold values from -0.09375 to 0.09375
- w_fgate: bfloat16 [4096, 16], P('kv', 'tp'), may hold values from -0.09375 to 0.09375
- bias_igate: float32 [16], P('tp'), may hold values from -1 to 1
- bias_fgate: float32 [16], P('tp'), may hold values from -1 to 4
- memory: float32 [512, 16, 128, 128], P(('dp', 'kv'), 'tp'), parts along dimension 0, may hold values from -0.8 to 0.8
- normalizer: float32 [512, 16, 128], P(('dp', 'kv'), 'tp'), parts along dimension 0, may hold values from -0.8 to 0.8
- stabilizer: float32 [512, 16], P(('dp', 'kv'), 'tp'), parts along dimension 0, may hold values from -1.5 to 1.5
- w_output: bfloat16 [2048, 4096], P('tp', 'kv'), may hold values from -0.125 to 0.125
- gain_mlp: float32 [4096], replicated, may hold values from 0.1 to 1.9
- w_gate: bfloat16 [4096, 11264], P(None, ('kv', 'tp')), may hold values from -0.09375 to 0.09375
- w_up: bfloat16 [4096, 11264], P(None, ('kv', 'tp')), may hold values from -0.09375 to 0.09375
- w_down: bfloat16 [11264, 4096], P(('kv', 'tp')), may hold values from -0.21875 to 0.21875
Outputs:
- mixed: bfloat16 [512, 4096], P('dp', ('kv', 'tp')), parts along dimension 0
- memory_next: float32 [512, 16, 128, 128], P(('dp', 'kv'), 'tp'), parts along dimension 0
- normalizer_next: float32 [512, 16, 128], P(('dp', 'kv'), 'tp'), parts along dimension 0
- stabilizer_next: float32 [512, 16], P(('dp', 'kv'), 'tp'), parts along dimension 0
There are 4 independent parts, one for each index of `dp`. A program takes and returns all parts, laid end to end along the dimension named above; an argument that names none is the same for every part. Nothing has to cross between parts.
All inputs are finite; a program needn't handle non-finite values.
Results may differ from a plain program's by a relative error of at most 0.014.
Values may be sent and summed in bfloat16 or wider, within the bound.
No kernel may reach another device: no remote copies, remote signals or barrier semaphores. Data moves between devices by JAX's collectives and lax.ppermute only.
A program may use at most 64 MiB of HBM per device.

v0:
```python
import jax
import jax.numpy as jnp
from jax import lax
from jax.experimental import pallas as pl
from jax.experimental.pallas import tpu as pltpu
from jax.sharding import Mesh
from jax.sharding import PartitionSpec as P


D = 4096
KV = ("kv_0", "kv_1")
DP_KV = ("dp", "kv_0", "kv_1")
KV_TP = ("kv_0", "kv_1", "tp")
Z, Y = 16, 4
ROWS = 128
HALF = 32
BLOCK = Z * HALF
epsilon = 1e-06
f32 = jnp.float32
bf16 = jnp.bfloat16


def exchanged(x, axis):
    return lax.all_to_all(x, axis, split_axis=0, concat_axis=0, tiled=True)


def swapped(x):
    return lax.ppermute(x, "tp", [(0, 1), (1, 0)])


def contracted(a, b, dim_a, dim_b):
    return lax.dot_general(a, b, (((dim_a,), (dim_b,)), ((), ())), preferred_element_type=f32)


def natural_row(i):
    return 8 * ((i // 2) % Z) + 2 * (i // 32) + i % 2


def final_row(i):
    return 8 * (i % Z) + 2 * ((i // Z) % Y) + i // 64


def row_selection(transposed, natural_row=natural_row):
    a = lax.broadcasted_iota(jnp.int32, (ROWS, ROWS), 0)
    b = lax.broadcasted_iota(jnp.int32, (ROWS, ROWS), 1)
    if transposed:
        hit = natural_row(a) == b
    else:
        hit = a == natural_row(b)
    return jnp.where(hit, 1.0, 0.0).astype(bf16)


def high_low(x):
    lane = lax.broadcasted_iota(jnp.int32, x.shape, 1)
    high = x.astype(bf16)
    low = (x - high.astype(f32)).astype(bf16)
    return jnp.where(lane < 64, high.astype(f32), low.astype(f32)).astype(bf16)


def column_of(row, count, offset=0):
    lane = lax.broadcasted_iota(jnp.int32, (count, row.shape[1]), 1)
    at = lax.broadcasted_iota(jnp.int32, (count, row.shape[1]), 0)
    return jnp.sum(jnp.where(lane == at + offset, row, 0.0), axis=1, keepdims=True)


def project_kernel(
    tok_ref, gain_ref, wi_ref, wf_ref, wq_ref, wk_ref, wv_ref, out_ref, w_ref, sems
):
    copies = [
        pltpu.make_async_copy(ref, w_ref.at[n], sems.at[n])
        for n, ref in enumerate((wq_ref, wk_ref, wv_ref))
    ]
    for copy in copies:
        copy.start()
    tok = jnp.dot(tok_ref[...], row_selection(False), preferred_element_type=f32)
    rows = contracted(row_selection(True), tok_ref[...], 1, 1).astype(bf16)
    out_ref[:, :, 3200:] = jnp.concatenate([rows, rows], axis=1).reshape(Y, 32, 128)
    scaled = (tok * column_of(gain_ref[...], 64)).astype(bf16)
    gates = jnp.concatenate([wi_ref[...].astype(f32), wf_ref[...].astype(f32)], axis=0)
    rest = jnp.zeros((48, 64), f32)
    gates = jnp.concatenate([gates, rest, gates, rest], axis=0).astype(bf16)
    extra = contracted(scaled, gates, 0, 1)
    squares = tok * tok
    high = squares.astype(bf16)
    low = (squares - high.astype(f32)).astype(bf16)
    lane = lax.broadcasted_iota(jnp.int32, (64, 128), 1)
    ones = jnp.where(lane % 64 == 16, 1.0, 0.0).astype(bf16)
    extra = extra + contracted(high, ones, 0, 0) + contracted(low, ones, 0, 0)
    out_ref[:, :, 3072:3200] = high_low(extra).reshape(Y, 32, 128)
    for n in range(3):
        copies[n].wait()
        part = contracted(scaled, w_ref[n], 0, 0).astype(bf16)
        out_ref[:, :, 1024 * n : 1024 * (n + 1)] = part.reshape(Y, 32, 1024)


def sum_y_kernel(in_ref, out_ref, tok_ref):
    for y in range(Y):
        tok_ref[:, 64 * y : 64 * (y + 1)] = in_ref[y, :, 3200:3264]
    for n in range(3):
        cut = slice(1024 * n, 1024 * (n + 1))
        total = in_ref[0, :, cut].astype(f32)
        for y in range(1, Y):
            total = total + in_ref[y, :, cut].astype(f32)
        out_ref[:, :, cut] = total.astype(bf16).reshape(Z, 2, 1024)
    total = in_ref[0, :, 3072:3200].astype(f32)
    for y in range(1, Y):
        total = total + in_ref[y, :, 3072:3200].astype(f32)
    total = total + jnp.concatenate([total[:, 64:], total[:, :64]], axis=1)
    out_ref[:, :, 3072:] = high_low(total).reshape(Z, 2, 128)


def by_head(x):
    count = x.shape[1]
    return jnp.concatenate(
        [jnp.broadcast_to(x[0:1], (8, count)), jnp.broadcast_to(x[1:2], (8, count))], axis=0
    )


def picked(x, offset):
    lane = lax.broadcasted_iota(jnp.int32, x.shape, 1)
    head = lax.broadcasted_iota(jnp.int32, x.shape, 0) % 8
    return jnp.sum(jnp.where(lane == head + offset, x, 0.0), axis=1, keepdims=True)


def cell_kernel(
    in_ref, bi_ref, bf_ref, mem_ref, norm_ref, stab_ref,
    hid_ref, mem_out_ref, norm_out_ref, stab_out_ref, rows_ref,
):
    sums = in_ref[0].astype(f32)
    for z in range(1, Z):
        sums = sums + in_ref[z].astype(f32)
    for n in range(3):
        for j in range(2):
            for h in range(8):
                at = 1024 * n + 128 * h
                rows_ref[n, 8 * j + h : 8 * j + h + 1, :] = sums[j : j + 1, at : at + 128]
    extra = by_head(sums[:, 3072:3136] + sums[:, 3136:3200])
    lane = lax.broadcasted_iota(jnp.int32, extra.shape, 1)
    total = jnp.sum(jnp.where(lane == 16, extra, 0.0), axis=1, keepdims=True)
    scaling = lax.rsqrt(total / D + epsilon)
    in_gate = scaling * picked(extra, 0) + picked(jnp.broadcast_to(bi_ref[...], (16, 8)), 0)
    forget = scaling * picked(extra, 8) + picked(jnp.broadcast_to(bf_ref[...], (16, 8)), 0)
    log_forget = jnp.minimum(forget, 0.0) - jnp.log1p(jnp.exp(-jnp.abs(forget)))
    kept = picked(by_head(stab_ref[...]), 0) + log_forget
    stab_next = jnp.maximum(kept, in_gate)
    keeping = jnp.exp(kept - stab_next)
    fresh = jnp.exp(in_gate - stab_next)
    queries = (scaling * rows_ref[0]).astype(bf16).astype(f32)
    keys = (scaling * rows_ref[1]).astype(bf16).astype(f32) * 128 ** (-0.5)
    values = (scaling * rows_ref[2]).astype(bf16).astype(f32)
    norm_next = keeping * norm_ref[...] + fresh * keys
    norm_out_ref[...] = norm_next
    denominator = jnp.sum(norm_next * queries, axis=1, keepdims=True)
    denominator = jnp.maximum(jnp.abs(denominator), jnp.exp(-stab_next))
    own = lax.broadcasted_iota(jnp.int32, (16, 8), 1)
    head = lax.broadcasted_iota(jnp.int32, (16, 8), 0) % 8
    spread = jnp.where(own == head, stab_next, 0.0)
    stab_out_ref[0:1, :] = jnp.sum(spread[:8], axis=0, keepdims=True)
    stab_out_ref[1:2, :] = jnp.sum(spread[8:], axis=0, keepdims=True)
    added = jnp.concatenate([fresh * values, jnp.zeros((112, 128), f32)], axis=0).T
    column = lax.broadcasted_iota(jnp.int32, (128, 128), 1)
    numerator = jnp.zeros((128, 128), f32)
    for i in range(16):
        update = added[:, i : i + 1] * keys[i : i + 1, :]
        mem_next = keeping[i : i + 1, :] * mem_ref[i] + update
        mem_out_ref[i] = mem_next
        read = jnp.sum(mem_next * queries[i : i + 1, :], axis=1, keepdims=True)
        numerator = jnp.where(column == i, read, numerator)
    hidden = (numerator.T[:16] / denominator).astype(bf16)
    for z in range(Z):
        hid_ref[2 * z] = hidden[:8]
        hid_ref[2 * z + 1] = hidden[8:]


def spread_kernel(in_ref, out_ref):
    for n in range(out_ref.shape[0]):
        out_ref[n] = in_ref[...]


def residual_kernel(
    place_ref, hid_ref, tok_ref, w0_ref, w1_ref, w2_ref, w3_ref, other_ref, spread_ref, parts_ref
):
    first = place_ref[0] == 0
    lower, upper = hid_ref[:, :1024], hid_ref[:, 1024:]
    own = jnp.where(first, lower, upper)
    other = jnp.where(first, upper, lower)
    for step, ref in enumerate((w0_ref, w1_ref, w2_ref, w3_ref)):
        part = contracted(own, ref[...], 1, 1).astype(bf16).astype(f32)
        part = part + contracted(other, other_ref[step], 1, 1).astype(bf16).astype(f32)
        parts_ref[(place_ref[2] + Y - step) % Y] = part
    branch = jnp.concatenate([parts_ref[y] for y in range(Y)], axis=1)
    at = lax.broadcasted_iota(jnp.int32, (Z, 32), 0)
    row = lax.broadcasted_iota(jnp.int32, (Z, 32), 1)
    chosen = jnp.where(row == 2 * at + place_ref[0], 1.0, 0.0).astype(bf16)
    tok = jnp.dot(chosen, tok_ref[...], preferred_element_type=f32)
    residual = (tok + branch).astype(bf16)
    for z in range(Z):
        spread_ref[z] = residual


def mlp_kernel(
    place_ref, own_ref, other_ref, gain_ref, wg_ref, wu_ref, wd_ref,
    keep_ref, send_ref, res_ref, x_ref, block_ref,
):
    first = place_ref[0] == 0
    squares = [jnp.zeros((Z, 256), f32) for _ in range(2 * Y)]
    for z in range(Z):
        gain = gain_ref[z : z + 1, :]
        for y in range(Y):
            own = own_ref[y, Z * z : Z * (z + 1), :].astype(f32)
            other = other_ref[y, Z * z : Z * (z + 1), :].astype(f32)
            for n, x in enumerate((jnp.where(first, own, other), jnp.where(first, other, own))):
                at = Y * n + y
                squares[at] = squares[at] + x * x
                x_ref[Z * at : Z * (at + 1), 256 * z : 256 * (z + 1)] = (x * gain).astype(bf16)
    total = jnp.sum(jnp.concatenate(squares, axis=0), axis=1, keepdims=True)
    scaling = lax.rsqrt(total / D + epsilon)
    scaling = jnp.broadcast_to(scaling, (ROWS, ROWS)).T[0:1]

    here = pl.multiple_of(Z * place_ref[3], Z)
    for y in range(Y):
        own = own_ref[y, pl.ds(here, Z), :]
        other = other_ref[y, pl.ds(here, Z), :]
        block_ref[Z * y : Z * (y + 1), :] = jnp.where(first, own, other)
        block_ref[64 + Z * y : 64 + Z * (y + 1), :] = jnp.where(first, other, own)
    at = lax.broadcasted_iota(jnp.int32, (HALF, 256), 0)
    lane = lax.broadcasted_iota(jnp.int32, (HALF, 256), 1)
    chosen = jnp.where(lane == at + place_ref[1], 1.0, 0.0).astype(bf16)
    res_ref[...] = contracted(chosen, block_ref[...], 1, 1).astype(bf16)

    x = x_ref[...]
    gate = scaling * contracted(wg_ref[...], x, 1, 1)
    up = scaling * contracted(wu_ref[...], x, 1, 1)
    activated = (gate * jax.nn.sigmoid(gate) * up).astype(bf16)
    for m in range(2 * Z):
        part = contracted(wd_ref[:, 128 * m : 128 * (m + 1)], activated, 0, 0)
        z = m // 2
        for pair in range(2):
            y = 2 * (m % 2) + pair
            lower = part[64 * pair : 64 * pair + HALF]
            upper = part[64 * pair + HALF : 64 * pair + 64]
            keep_ref[y, HALF * z : HALF * (z + 1), :] = jnp.where(first, lower, upper)
            send_ref[y, HALF * z : HALF * (z + 1), :] = jnp.where(first, upper, lower).astype(bf16)


def finish_kernel(in_ref, res_ref, out_ref):
    total = res_ref[...].astype(f32)
    acc = in_ref[0].astype(f32)
    for z in range(1, Z):
        acc = acc + in_ref[z].astype(f32)
    mixed = (total + acc).astype(bf16)
    out_ref[...] = jnp.dot(mixed, row_selection(True, final_row), preferred_element_type=f32).astype(bf16)


def called(kernel, out_shape, flops=0, grant=16, **kw):
    return pl.pallas_call(
        kernel,
        out_shape=out_shape,
        cost_estimate=pl.CostEstimate(flops=flops, bytes_accessed=10**6, transcendentals=0),
        compiler_params=pltpu.CompilerParams(vmem_limit_bytes=grant * 2**20),
        **kw,
    )


IN_VMEM = pl.BlockSpec(memory_space=pltpu.VMEM)
IN_SMEM = pl.BlockSpec(memory_space=pltpu.SMEM)
IN_HBM = pl.BlockSpec(memory_space=pltpu.HBM)


def layer(
    tokens,
    gain_mix,
    w_query,
    w_key,
    w_value,
    w_igate,
    w_fgate,
    bias_igate,
    bias_fgate,
    memory,
    normalizer,
    stabilizer,
    w_output,
    gain_mlp,
    w_gate,
    w_up,
    w_down,
):
    core = lax.axis_index("tp")
    at_z, at_y = lax.axis_index("kv_0"), lax.axis_index("kv_1")
    place = jnp.stack([core, 64 * at_y + HALF * core, at_y, at_z]).astype(jnp.int32)
    shape = jax.ShapeDtypeStruct
    partials = called(
        project_kernel,
        shape((Y, 32, 3328), bf16),
        flops=2 * 64 * 128 * 3200,
        grant=60,
        in_specs=[IN_VMEM] * 4 + [IN_HBM] * 3,
        scratch_shapes=[pltpu.VMEM((3, 64, 1024), bf16), pltpu.SemaphoreType.DMA((3,))],
    )(tokens.T, gain_mix.reshape(1, 64), w_igate.T, w_fgate.T, w_query, w_key, w_value)
    w_own = w_output.T
    partials = exchanged(partials, "kv_1")
    partials, tok = called(
        sum_y_kernel, (shape((Z, 2, 3200), bf16), shape((32, 256), bf16)), flops=10**6
    )(partials)
    partials = exchanged(partials, "kv_0")
    w_all = [w_own]
    for step in range(1, Y):
        w_all.append(lax.ppermute(w_own, "kv_1", [(i, (i + step) % Y) for i in range(Y)]))
    w_other = swapped(jnp.stack(w_all))
    hidden, memory_next, norm_next, stab_next = called(
        cell_kernel,
        (
            shape((2 * Z, 8, 128), bf16),
            shape((16, 128, 128), f32),
            shape((16, 128), f32),
            shape((2, 8), f32),
        ),
        flops=10**7,
        scratch_shapes=[pltpu.VMEM((3, 16, 128), f32)],
    )(
        partials,
        bias_igate.reshape(1, 8),
        bias_fgate.reshape(1, 8),
        memory.reshape(16, 128, 128),
        normalizer.reshape(16, 128),
        stabilizer,
    )
    hidden = exchanged(hidden, ("kv_0", "tp"))
    spread = called(
        residual_kernel,
        shape((Z, Z, 256), bf16),
        flops=10**7,
        in_specs=[IN_SMEM] + [IN_VMEM] * 7,
        scratch_shapes=[pltpu.VMEM((Y, Z, 64), f32)],
    )(place, hidden.reshape(Z, 2048), tok, *w_all, w_other)
    spread = exchanged(spread, "kv_0").reshape(256, 256)
    spread = called(spread_kernel, shape((Y, 256, 256), bf16), flops=10**6)(spread)
    spread = exchanged(spread, "kv_1")
    other = swapped(spread)
    keep, send, residual = called(
        mlp_kernel,
        (
            shape((Y, BLOCK, ROWS), f32),
            shape((Y, BLOCK, ROWS), bf16),
            shape((HALF, ROWS), bf16),
        ),
        flops=6 * 128 * 88 * 4096,
        in_specs=[IN_SMEM] + [IN_VMEM] * 6,
        scratch_shapes=[pltpu.VMEM((ROWS, D), bf16), pltpu.VMEM((ROWS, 256), bf16)],
    )(place, spread, other, gain_mlp.reshape(Z, 256), w_gate.T, w_up.T, w_down)
    terms = (keep + swapped(send).astype(f32)).astype(bf16)
    terms = exchanged(terms, "kv_1").astype(f32).sum(axis=0).astype(bf16)
    terms = exchanged(terms.reshape(Z, HALF, ROWS), "kv_0")
    mixed = called(finish_kernel, shape((HALF, ROWS), bf16), flops=10**6)(terms, residual)
    return (
        mixed.T,
        memory_next.reshape(2, 8, 128, 128),
        norm_next.reshape(2, 8, 128),
        stab_next,
    )


def solution(mesh):
    torus = Mesh(
        mesh.devices.reshape(mesh.shape["dp"], Z, Y, mesh.shape["tp"]),
        ("dp", "kv_0", "kv_1", "tp"),
    )
    in_specs = (
        P("dp", KV),
        P(KV),
        P(KV, "tp"),
        P(KV, "tp"),
        P(KV, "tp"),
        P(KV, "tp"),
        P(KV, "tp"),
        P("tp"),
        P("tp"),
        P(DP_KV, "tp", None, None),
        P(DP_KV, "tp", None),
        P(DP_KV, "tp"),
        P("tp", KV),
        P(),
        P(None, KV_TP),
        P(None, KV_TP),
        P(KV_TP, None),
    )
    out_specs = (P("dp", KV_TP), P(DP_KV, "tp", None, None), P(DP_KV, "tp", None), P(DP_KV, "tp"))
    return jax.shard_map(layer, mesh=torus, in_specs=in_specs, out_specs=out_specs, check_vma=False)
```

profile of v0, /device:TPU:1, one launch (start us, length us, event | category | flops | bytes accessed | tf_op | source)
XLA Modules:
  0.0 151.7 jit_solution(6885198768794301983)
XLA Ops:
  0.6 3.2 %shard_map.192 = bf16[4,32,3328]{2,1,0:T(8,128)(2,1)} custom-call(bf16[64,128]{1,0:T(8,128)(2,1)} %bitcast.41, f32[1,64]{1,0:T(1,128)} %bitcast.45, bf16[8,64]{1,0:T(8,128)(2,1)} %bitcast.43, bf16[8,64]{1,0:T(8,128)(2,1)} %bitcast.44, bf16[64,1024]{1,0:T(8,128)(2,1)} %wq_ref.1, bf16[64,1024]{1,0:T(8,128)(2,1)} %wk_ref.1, bf16[64,1024]{1,0:T(8,128)(2,1)} %wv_ref.1), custom_call_target="tpu_custom_call" | custom-call | flops 52428800 | bytes 1000000 | tf_op jit(solution)/shard_map/pallas_call | solution.py:293
  3.9 13.7 %all_to_all.35.in_ref = bf16[4,32,3328]{2,1,0:T(8,128)(2,1)S(1)} all-to-all(bf16[4,32,3328]{2,1,0:T(8,128)(2,1)} %shard_map.192), channel_id=1, replica_groups=mesh['dp'=4,'kv_0'=16,'kv_1'=4,'tp'=2] {'kv_1'}, dimensions={0} | all-to-all | bytes 1703936 | tf_op jit(solution)/shard_map/all_to_all | solution.py:24
  17.6 0.0 copy-start
  17.6 0.8 shard_map.193
  18.4 0.0 copy-start.4
  18.4 18.2 %all-to-all-start.1 = ((bf16[16,2,3200]{2,1,0:T(2,128)(2,1)}), bf16[16,2,3200]{2,1,0:T(2,128)(2,1)S(1)}, u32[]{:S(2)}, u32[]{:S(2)}) async-start(bf16[16,2,3200]{2,1,0:T(2,128)(2,1)} %get-tuple-element.13), calls=%async_computation.1 | async-start | bytes 409600 | tf_op jit(solution)/shard_map/all_to_all | solution.py:24
  36.6 0.0 copy-done.4
  36.6 2.8 %collective-permute-start.2 = (bf16[64,1024]{1,0:T(8,128)(2,1)S(1)}, bf16[64,1024]{1,0:T(8,128)(2,1)S(1)}, u32[]{:S(2)}, u32[]{:S(2)}) collective-permute-start(bf16[64,1024]{1,0:T(8,128)(2,1)S(1)} %bitcast.29), channel_id=1, source_target_pairs={{0,6},{2,0},{4,2},{6,4},{1,7},{3,1},{5,3},{7,5},{8,14},{10,8},{12,... | collective-permute-start | bytes 393224 | tf_op jit(solution)/shard_map/ppermute | solution.py:309
  39.4 3.1 %collective-permute-start.1 = (bf16[64,1024]{1,0:T(8,128)(2,1)S(1)}, bf16[64,1024]{1,0:T(8,128)(2,1)S(1)}, u32[]{:S(2)}, u32[]{:S(2)}) collective-permute-start(bf16[64,1024]{1,0:T(8,128)(2,1)S(1)} %bitcast.30), channel_id=1, source_target_pairs={{0,4},{2,6},{4,0},{6,2},{1,5},{3,7},{5,1},{7,3},{8,12},{10,14},{12... | collective-permute-start | bytes 393224 | tf_op jit(solution)/shard_map/ppermute | solution.py:309
  42.5 1.9 %collective-permute-start = (bf16[64,1024]{1,0:T(8,128)(2,1)S(1)}, bf16[64,1024]{1,0:T(8,128)(2,1)S(1)}, u32[]{:S(2)}, u32[]{:S(2)}) collective-permute-start(bf16[64,1024]{1,0:T(8,128)(2,1)S(1)} %bitcast.31), channel_id=1, source_target_pairs={{0,2},{2,4},{4,6},{6,0},{1,3},{3,5},{5,7},{7,1},{8,10},{10,12},{12... | collective-permute-start | bytes 393224 | tf_op jit(solution)/shard_map/ppermute | solution.py:309
  44.4 0.0 collective-permute-done.2.w3_ref
  44.4 2.5 %collective-permute-done.1.w2_ref = bf16[64,1024]{1,0:T(8,128)(2,1)S(1)} collective-permute-done((bf16[64,1024]{1,0:T(8,128)(2,1)S(1)}, bf16[64,1024]{1,0:T(8,128)(2,1)S(1)}, u32[]{:S(2)}, u32[]{:S(2)}) %collective-permute-start.1) | collective-permute-done | bytes 131104 | tf_op jit(solution)/shard_map/ppermute | solution.py:309
  46.9 3.9 %collective-permute-done.w1_ref = bf16[64,1024]{1,0:T(8,128)(2,1)S(1)} collective-permute-done((bf16[64,1024]{1,0:T(8,128)(2,1)S(1)}, bf16[64,1024]{1,0:T(8,128)(2,1)S(1)}, u32[]{:S(2)}, u32[]{:S(2)}) %collective-permute-start) | collective-permute-done | bytes 131104 | tf_op jit(solution)/shard_map/ppermute | solution.py:309
  50.8 0.0 copy-start.5
  50.8 0.1 pad_maximum_fusion
  50.9 4.6 %collective-permute-start.3 = (bf16[4,64,1024]{2,1,0:T(8,128)(2,1)S(1)}, bf16[4,64,1024]{2,1,0:T(8,128)(2,1)S(1)}, u32[]{:S(2)}, u32[]{:S(2)}) collective-permute-start(bf16[4,64,1024]{2,1,0:T(8,128)(2,1)S(1)} %pad_maximum_fusion), channel_id=1, source_target_pairs={{0,1},{1,0},{2,3},{3,2},{4,5},{5,4},{6,7},{7,6},{8,9},{9,8},{10,11... | collective-permute-start | bytes 1572872 | tf_op jit(solution)/shard_map/ppermute | solution.py:28
  55.5 0.0 all-to-all-done.1.in_ref
  55.5 0.0 copy-start.6
  55.5 0.0 copy-start.7
  55.6 0.0 copy-done
  55.6 0.0 copy-done.5
  55.6 0.0 copy-done.8
  55.6 0.6 copy-done.6
  56.2 0.0 copy-done.7
  56.2 2.6 %shard_map.194 = (bf16[32,8,128]{2,1,0:T(8,128)(2,1)}, f32[16,128,128]{2,1,0:T(8,128)}, f32[16,128]{1,0:T(8,128)}, f32[2,8]{1,0:T(2,128)}) custom-call(bf16[16,2,3200]{2,1,0:T(2,128)(2,1)S(1)} %all-to-all-done.1.in_ref, f32[1,8]{1,0:T(1,128)S(1)} %bitcast.38, f32[1,8]{1,0:T(1,128)S(1)} %bitcast.39, f32[16,128,128]{2,1,0:T(8,128)S(1)} %bitcast.25, ...), custom_call_target="tpu_custom_call" | custom-call | flops 10000000 | bytes 1000000 | tf_op jit(solution)/shard_map/pallas_call | solution.py:311
  58.9 12.2 %all-to-all-start.2 = ((bf16[32,8,128]{2,1,0:T(8,128)(2,1)}), bf16[32,8,128]{2,1,0:T(8,128)(2,1)S(1)}, u32[]{:S(2)}, u32[]{:S(2)}) async-start(bf16[32,8,128]{2,1,0:T(8,128)(2,1)} %get-tuple-element.14), calls=%async_computation.2 | async-start | bytes 131072 | tf_op jit(solution)/shard_map/all_to_all | solution.py:24
  71.0 0.1 pad_add_fusion.place_ref
  71.1 12.9 %all-to-all-done.2 = bf16[32,8,128]{2,1,0:T(8,128)(2,1)S(1)} async-done(((bf16[32,8,128]{2,1,0:T(8,128)(2,1)}), bf16[32,8,128]{2,1,0:T(8,128)(2,1)S(1)}, u32[]{:S(2)}, u32[]{:S(2)}) %all-to-all-start.2) | async-done | bytes 65568 | tf_op jit(solution)/shard_map/all_to_all | solution.py:24
  84.1 0.0 collective-permute-done.3.other_ref
  84.1 0.0 copy-start.3
  84.1 1.0 shard_map.195
  85.1 14.6 %all_to_all.36 = bf16[16,16,256]{2,1,0:T(8,128)(2,1)S(1)} all-to-all(bf16[16,16,256]{2,1,0:T(8,128)(2,1)S(1)} %shard_map.195), channel_id=1, replica_groups=mesh['dp'=4,'kv_0'=16,'kv_1'=4,'tp'=2] {'kv_0'}, dimensions={0} | all-to-all | bytes 262144 | tf_op jit(solution)/shard_map/all_to_all | solution.py:24
  99.8 0.0 copy-start.9
  99.8 9.5 %all_to_all.37.own_ref = bf16[4,256,256]{2,1,0:T(8,128)(2,1)S(1)} all-to-all(bf16[4,256,256]{2,1,0:T(8,128)(2,1)S(1)} %shard_map.196), channel_id=1, replica_groups=mesh['dp'=4,'kv_0'=16,'kv_1'=4,'tp'=2] {'kv_1'}, dimensions={0} | all-to-all | bytes 1048576 | tf_op jit(solution)/shard_map/all_to_all | solution.py:24
  109.2 6.8 %collective-permute-start.4 = (bf16[4,256,256]{2,1,0:T(8,128)(2,1)S(1)}, bf16[4,256,256]{2,1,0:T(8,128)(2,1)S(1)}, u32[]{:S(2)}, u32[]{:S(2)}) collective-permute-start(bf16[4,256,256]{2,1,0:T(8,128)(2,1)S(1)} %all_to_all.37.own_ref), channel_id=1, source_target_pairs={{0,1},{1,0},{2,3},{3,2},{4,5},{5,4},{6,7},{7,6},{8,9},{9,8},{10,11... | collective-permute-start | bytes 1572872 | tf_op jit(solution)/shard_map/ppermute | solution.py:28
  116.0 0.0 copy-done.9
  116.0 1.5 collective-permute-done.4.other_ref
  117.5 0.0 copy-done.3
  117.5 0.0 copy-done.1
  117.5 0.0 copy-done.2
  117.5 1.9 %shard_map.197 = (f32[4,512,128]{2,1,0:T(8,128)S(1)}, bf16[4,512,128]{2,1,0:T(8,128)(2,1)S(1)}, bf16[32,128]{1,0:T(8,128)(2,1)S(1)}) custom-call(s32[4]{0:T(128)S(1)} %pad_add_fusion.place_ref, bf16[4,256,256]{2,1,0:T(8,128)(2,1)S(1)} %all_to_all.37.own_ref, bf16[4,256,256]{2,1,0:T(8,128)(2,1)S(1)} %collective-permute-done.4.other_ref, ...), custom_call_target="tpu_custom_call" | custom-call | flops 276824064 | bytes 1000000 | tf_op jit(solution)/shard_map/pallas_call | solution.py:341
  119.4 2.3 %collective-permute-start.5 = (bf16[4,512,128]{2,1,0:T(8,128)(2,1)S(1)}, bf16[4,512,128]{2,1,0:T(8,128)(2,1)S(1)}, u32[]{:S(2)}, u32[]{:S(2)}) collective-permute-start(bf16[4,512,128]{2,1,0:T(8,128)(2,1)S(1)} %get-tuple-element.17), channel_id=1, source_target_pairs={{0,1},{1,0},{2,3},{3,2},{4,5},{5,4},{6,7},{7,6},{8,9},{9,8},{10,11... | collective-permute-start | bytes 1572872 | tf_op jit(solution)/shard_map/ppermute | solution.py:28
  121.7 1.5 collective-permute-done.5
  123.2 0.1 add_convert_fusion
  123.3 11.6 %all_to_all.38 = bf16[4,512,128]{2,1,0:T(8,128)(2,1)S(1)} all-to-all(bf16[4,512,128]{2,1,0:T(8,128)(2,1)S(1)} %add_convert_fusion), channel_id=1, replica_groups=mesh['dp'=4,'kv_0'=16,'kv_1'=4,'tp'=2] {'kv_1'}, dimensions={0} | all-to-all | bytes 1048576 | tf_op jit(solution)/shard_map/all_to_all | solution.py:24
  134.9 0.1 reduce_sum.12
  135.0 15.9 %all_to_all.39.in_ref = bf16[16,32,128]{2,1,0:T(8,128)(2,1)S(1)} all-to-all(bf16[16,32,128]{2,1,0:T(8,128)(2,1)S(1)} %bitcast.40), channel_id=1, replica_groups=mesh['dp'=4,'kv_0'=16,'kv_1'=4,'tp'=2] {'kv_0'}, dimensions={0} | all-to-all | bytes 262144 | tf_op jit(solution)/shard_map/all_to_all | solution.py:24
  150.9 0.8 shard_map.198
  (6 shorter events, 0.1 us)
Async XLA Ops:
  17.6 38.0 %copy-start = (f32[2,8,128,128]{3,2,1,0:T(8,128)S(1)}, f32[2,8,128,128]{3,2,1,0:T(8,128)}, u32[]{:S(2)}) copy-start(f32[2,8,128,128]{3,2,1,0:T(8,128)} %param.26) | copy-start | bytes 3145732
  18.4 18.2 %copy-start.4 = (bf16[1024,64]{0,1:T(8,128)(2,1)S(1)}, bf16[1024,64]{0,1:T(8,128)(2,1)}, u32[]{:S(2)}) copy-start(bf16[1024,64]{0,1:T(8,128)(2,1)} %param.29) | copy-start | bytes 393220
  18.4 37.1 %all-to-all-start.1 = ((bf16[16,2,3200]{2,1,0:T(2,128)(2,1)}), bf16[16,2,3200]{2,1,0:T(2,128)(2,1)S(1)}, u32[]{:S(2)}, u32[]{:S(2)}) async-start(bf16[16,2,3200]{2,1,0:T(2,128)(2,1)} %get-tuple-element.13), calls=%async_computation.1 | async-start | bytes 409600 | tf_op jit(solution)/shard_map/all_to_all | solution.py:24
  36.6 7.8 %collective-permute-start.2 = (bf16[64,1024]{1,0:T(8,128)(2,1)S(1)}, bf16[64,1024]{1,0:T(8,128)(2,1)S(1)}, u32[]{:S(2)}, u32[]{:S(2)}) collective-permute-start(bf16[64,1024]{1,0:T(8,128)(2,1)S(1)} %bitcast.29), channel_id=1, source_target_pairs={{0,6},{2,0},{4,2},{6,4},{1,7},{3,1},{5,3},{7,5},{8,14},{10,8},{12,... | collective-permute-start | bytes 393224 | tf_op jit(solution)/shard_map/ppermute | solution.py:309
  39.4 7.5 %collective-permute-start.1 = (bf16[64,1024]{1,0:T(8,128)(2,1)S(1)}, bf16[64,1024]{1,0:T(8,128)(2,1)S(1)}, u32[]{:S(2)}, u32[]{:S(2)}) collective-permute-start(bf16[64,1024]{1,0:T(8,128)(2,1)S(1)} %bitcast.30), channel_id=1, source_target_pairs={{0,4},{2,6},{4,0},{6,2},{1,5},{3,7},{5,1},{7,3},{8,12},{10,14},{12... | collective-permute-start | bytes 393224 | tf_op jit(solution)/shard_map/ppermute | solution.py:309
  42.5 8.3 %collective-permute-start = (bf16[64,1024]{1,0:T(8,128)(2,1)S(1)}, bf16[64,1024]{1,0:T(8,128)(2,1)S(1)}, u32[]{:S(2)}, u32[]{:S(2)}) collective-permute-start(bf16[64,1024]{1,0:T(8,128)(2,1)S(1)} %bitcast.31), channel_id=1, source_target_pairs={{0,2},{2,4},{4,6},{6,0},{1,3},{3,5},{5,7},{7,1},{8,10},{10,12},{12... | collective-permute-start | bytes 393224 | tf_op jit(solution)/shard_map/ppermute | solution.py:309
  50.8 4.8 %copy-start.5 = (f32[2,8,128]{2,1,0:T(8,128)S(1)}, f32[2,8,128]{2,1,0:T(8,128)}, u32[]{:S(2)}) copy-start(f32[2,8,128]{2,1,0:T(8,128)} %param.27) | copy-start | bytes 24580
  50.8 4.8 %copy-start.8 = (f32[8]{0:T(128)S(1)}, f32[8]{0:T(128)}, u32[]{:S(2)}) copy-start(f32[8]{0:T(128)} %param.25) | copy-start | bytes 100
  50.9 33.2 %collective-permute-start.3 = (bf16[4,64,1024]{2,1,0:T(8,128)(2,1)S(1)}, bf16[4,64,1024]{2,1,0:T(8,128)(2,1)S(1)}, u32[]{:S(2)}, u32[]{:S(2)}) collective-permute-start(bf16[4,64,1024]{2,1,0:T(8,128)(2,1)S(1)} %pad_maximum_fusion), channel_id=1, source_target_pairs={{0,1},{1,0},{2,3},{3,2},{4,5},{5,4},{6,7},{7,6},{8,9},{9,8},{10,11... | collective-permute-start | bytes 1572872 | tf_op jit(solution)/shard_map/ppermute | solution.py:28
  55.5 0.7 copy-start.6
  55.5 0.7 copy-start.7
  58.9 25.2 %all-to-all-start.2 = ((bf16[32,8,128]{2,1,0:T(8,128)(2,1)}), bf16[32,8,128]{2,1,0:T(8,128)(2,1)S(1)}, u32[]{:S(2)}, u32[]{:S(2)}) async-start(bf16[32,8,128]{2,1,0:T(8,128)(2,1)} %get-tuple-element.14), calls=%async_computation.2 | async-start | bytes 131072 | tf_op jit(solution)/shard_map/all_to_all | solution.py:24
  84.1 33.4 %copy-start.3 = (bf16[88,4096]{1,0:T(8,128)(2,1)S(1)}, bf16[88,4096]{1,0:T(8,128)(2,1)}, u32[]{:S(2)}) copy-start(bf16[88,4096]{1,0:T(8,128)(2,1)} %wd_ref.1) | copy-start | bytes 2162692
  99.7 17.8 %copy-start.1 = (bf16[4096,88]{0,1:T(8,128)(2,1)S(1)}, bf16[4096,88]{0,1:T(8,128)(2,1)}, u32[]{:S(2)}) copy-start(bf16[4096,88]{0,1:T(8,128)(2,1)} %param.31) | copy-start | bytes 2162692
  99.7 17.8 %copy-start.2 = (bf16[4096,88]{0,1:T(8,128)(2,1)S(1)}, bf16[4096,88]{0,1:T(8,128)(2,1)}, u32[]{:S(2)}) copy-start(bf16[4096,88]{0,1:T(8,128)(2,1)} %param.32) | copy-start | bytes 2162692
  99.8 16.3 %copy-start.9 = (f32[4096]{0:T(1024)S(1)}, f32[4096]{0:T(1024)}, u32[]{:S(2)}) copy-start(f32[4096]{0:T(1024)} %param.30) | copy-start | bytes 49156
  109.2 8.3 %collective-permute-start.4 = (bf16[4,256,256]{2,1,0:T(8,128)(2,1)S(1)}, bf16[4,256,256]{2,1,0:T(8,128)(2,1)S(1)}, u32[]{:S(2)}, u32[]{:S(2)}) collective-permute-start(bf16[4,256,256]{2,1,0:T(8,128)(2,1)S(1)} %all_to_all.37.own_ref), channel_id=1, source_target_pairs={{0,1},{1,0},{2,3},{3,2},{4,5},{5,4},{6,7},{7,6},{8,9},{9,8},{10,11... | collective-permute-start | bytes 1572872 | tf_op jit(solution)/shard_map/ppermute | solution.py:28
  119.4 3.8 %collective-permute-start.5 = (bf16[4,512,128]{2,1,0:T(8,128)(2,1)S(1)}, bf16[4,512,128]{2,1,0:T(8,128)(2,1)S(1)}, u32[]{:S(2)}, u32[]{:S(2)}) collective-permute-start(bf16[4,512,128]{2,1,0:T(8,128)(2,1)S(1)} %get-tuple-element.17), channel_id=1, source_target_pairs={{0,1},{1,0},{2,3},{3,2},{4,5},{5,4},{6,7},{7,6},{8,9},{9,8},{10,11... | collective-permute-start | bytes 1572872 | tf_op jit(solution)/shard_map/ppermute | solution.py:28
where the time goes:
time: 155 us; the launch traced here: 152 us
  blocking collectives  65.3 us (42%)
  starting transfers between devices  51.9 us (33%)
  waiting for transfers between devices  22.3 us (14%)
  Pallas kernels  10.4 us (7%)
    all_to_all x5, blocking collectives, exchanged(): return lax.all_to_all(x, axis, split_axis=0, concat_axis=0, tiled=True)  65.3 us
    all_to_all x2, starting transfers between devices, exchanged(): return lax.all_to_all(x, axis, split_axis=0, concat_axis=0, tiled=True)  30.4 us
    ppermute x3, starting transfers between devices, swapped(): return lax.ppermute(x, 'tp', [(0, 1), (1, 0)])  13.7 us
    all_to_all x2, waiting for transfers between devices, exchanged(): return lax.all_to_all(x, axis, split_axis=0, concat_axis=0, tiled=True)  12.9 us
    ppermute x3, starting transfers between devices, layer(): lax.ppermute(w_own, 'kv_1', [(i, (i + step) % Y) for i in range(Y)])  7.81 us
    ppermute x3, waiting for transfers between devices, layer(): lax.ppermute(w_own, 'kv_1', [(i, (i + step) % Y) for i in range(Y)])  6.36 us
    pallas_call x1, Pallas kernels, layer(): called(project_kernel, shape((Y, 32, 3328), bf16), flops=2 * 64 * 128 * 3...  3.22 us
  transfers between devices with their start and end apart: 8, of which 5 were waited for; matrix products, arithmetic and copies ran while one was open for 0% of the time, Pallas kernels for 2%

commit v1 on v0

--- a/solution.py
+++ b/solution.py
@@ -24,6 +24,13 @@
     return lax.all_to_all(x, axis, split_axis=0, concat_axis=0, tiled=True)
 
 
+def mirrored(x):
+    groups = [[0, 2, 4, 6], [7, 5, 3, 1]]
+    return lax.all_to_all(
+        x, ("kv_1", "tp"), split_axis=0, concat_axis=0, tiled=True, axis_index_groups=groups
+    )
+
+
 def swapped(x):
     return lax.ppermute(x, "tp", [(0, 1), (1, 0)])
 
@@ -64,14 +71,8 @@
 
 
 def project_kernel(
-    tok_ref, gain_ref, wi_ref, wf_ref, wq_ref, wk_ref, wv_ref, out_ref, w_ref, sems
-):
-    copies = [
-        pltpu.make_async_copy(ref, w_ref.at[n], sems.at[n])
-        for n, ref in enumerate((wq_ref, wk_ref, wv_ref))
-    ]
-    for copy in copies:
-        copy.start()
+    tok_ref, gain_ref, wi_ref, wf_ref, wq_ref, wk_ref, wv_ref, out_ref
+):
     tok = jnp.dot(tok_ref[...], row_selection(False), preferred_element_type=f32)
     rows = contracted(row_selection(True), tok_ref[...], 1, 1).astype(bf16)
     out_ref[:, :, 3200:] = jnp.concatenate([rows, rows], axis=1).reshape(Y, 32, 128)
@@ -87,9 +88,8 @@
     ones = jnp.where(lane % 64 == 16, 1.0, 0.0).astype(bf16)
     extra = extra + contracted(high, ones, 0, 0) + contracted(low, ones, 0, 0)
     out_ref[:, :, 3072:3200] = high_low(extra).reshape(Y, 32, 128)
-    for n in range(3):
-        copies[n].wait()
-        part = contracted(scaled, w_ref[n], 0, 0).astype(bf16)
+    for n, ref in enumerate((wq_ref, wk_ref, wv_ref)):
+        part = contracted(scaled, ref[...], 0, 0).astype(bf16)
         out_ref[:, :, 1024 * n : 1024 * (n + 1)] = part.reshape(Y, 32, 1024)
 
 
@@ -123,7 +123,7 @@
 
 
 def cell_kernel(
-    in_ref, bi_ref, bf_ref, mem_ref, norm_ref, stab_ref,
+    in_ref, small_ref, mem_ref, norm_ref,
     hid_ref, mem_out_ref, norm_out_ref, stab_out_ref, rows_ref,
 ):
     sums = in_ref[0].astype(f32)
@@ -138,10 +138,10 @@
     lane = lax.broadcasted_iota(jnp.int32, extra.shape, 1)
     total = jnp.sum(jnp.where(lane == 16, extra, 0.0), axis=1, keepdims=True)
     scaling = lax.rsqrt(total / D + epsilon)
-    in_gate = scaling * picked(extra, 0) + picked(jnp.broadcast_to(bi_ref[...], (16, 8)), 0)
-    forget = scaling * picked(extra, 8) + picked(jnp.broadcast_to(bf_ref[...], (16, 8)), 0)
+    in_gate = scaling * picked(extra, 0) + picked(jnp.broadcast_to(small_ref[2:3, :], (16, 8)), 0)
+    forget = scaling * picked(extra, 8) + picked(jnp.broadcast_to(small_ref[3:4, :], (16, 8)), 0)
     log_forget = jnp.minimum(forget, 0.0) - jnp.log1p(jnp.exp(-jnp.abs(forget)))
-    kept = picked(by_head(stab_ref[...]), 0) + log_forget
+    kept = picked(by_head(small_ref[0:2, :]), 0) + log_forget
     stab_next = jnp.maximum(kept, in_gate)
     keeping = jnp.exp(kept - stab_next)
     fresh = jnp.exp(in_gate - stab_next)
@@ -203,12 +203,14 @@
     keep_ref, send_ref, res_ref, x_ref, block_ref,
 ):
     first = place_ref[0] == 0
+    mine = [jnp.where(first, y, Y - 1 - y) for y in range(Y)]
+    theirs = [jnp.where(first, Y - 1 - y, y) for y in range(Y)]
     squares = [jnp.zeros((Z, 256), f32) for _ in range(2 * Y)]
     for z in range(Z):
         gain = gain_ref[z : z + 1, :]
         for y in range(Y):
-            own = own_ref[y, Z * z : Z * (z + 1), :].astype(f32)
-            other = other_ref[y, Z * z : Z * (z + 1), :].astype(f32)
+            own = own_ref[mine[y], Z * z : Z * (z + 1), :].astype(f32)
+            other = other_ref[theirs[y], Z * z : Z * (z + 1), :].astype(f32)
             for n, x in enumerate((jnp.where(first, own, other), jnp.where(first, other, own))):
                 at = Y * n + y
                 squares[at] = squares[at] + x * x
@@ -219,8 +221,8 @@
 
     here = pl.multiple_of(Z * place_ref[3], Z)
     for y in range(Y):
-        own = own_ref[y, pl.ds(here, Z), :]
-        other = other_ref[y, pl.ds(here, Z), :]
+        own = own_ref[mine[y], pl.ds(here, Z), :]
+        other = other_ref[theirs[y], pl.ds(here, Z), :]
         block_ref[Z * y : Z * (y + 1), :] = jnp.where(first, own, other)
         block_ref[64 + Z * y : 64 + Z * (y + 1), :] = jnp.where(first, other, own)
     at = lax.broadcasted_iota(jnp.int32, (HALF, 256), 0)
@@ -239,8 +241,8 @@
             y = 2 * (m % 2) + pair
             lower = part[64 * pair : 64 * pair + HALF]
             upper = part[64 * pair + HALF : 64 * pair + 64]
-            keep_ref[y, HALF * z : HALF * (z + 1), :] = jnp.where(first, lower, upper)
-            send_ref[y, HALF * z : HALF * (z + 1), :] = jnp.where(first, upper, lower).astype(bf16)
+            keep_ref[mine[y], HALF * z : HALF * (z + 1), :] = jnp.where(first, lower, upper)
+            send_ref[theirs[y], HALF * z : HALF * (z + 1), :] = jnp.where(first, upper, lower).astype(bf16)
 
 
 def finish_kernel(in_ref, res_ref, out_ref):
@@ -264,7 +266,6 @@
 
 IN_VMEM = pl.BlockSpec(memory_space=pltpu.VMEM)
 IN_SMEM = pl.BlockSpec(memory_space=pltpu.SMEM)
-IN_HBM = pl.BlockSpec(memory_space=pltpu.HBM)
 
 
 def layer(
@@ -295,8 +296,6 @@
         shape((Y, 32, 3328), bf16),
         flops=2 * 64 * 128 * 3200,
         grant=60,
-        in_specs=[IN_VMEM] * 4 + [IN_HBM] * 3,
-        scratch_shapes=[pltpu.VMEM((3, 64, 1024), bf16), pltpu.SemaphoreType.DMA((3,))],
     )(tokens.T, gain_mix.reshape(1, 64), w_igate.T, w_fgate.T, w_query, w_key, w_value)
     w_own = w_output.T
     partials = exchanged(partials, "kv_1")
@@ -308,6 +307,9 @@
     for step in range(1, Y):
         w_all.append(lax.ppermute(w_own, "kv_1", [(i, (i + step) % Y) for i in range(Y)]))
     w_other = swapped(jnp.stack(w_all))
+    small = jnp.concatenate(
+        [stabilizer, bias_igate.reshape(1, 8), bias_fgate.reshape(1, 8)], axis=0
+    )
     hidden, memory_next, norm_next, stab_next = called(
         cell_kernel,
         (
@@ -319,12 +321,7 @@
         flops=10**7,
         scratch_shapes=[pltpu.VMEM((3, 16, 128), f32)],
     )(
-        partials,
-        bias_igate.reshape(1, 8),
-        bias_fgate.reshape(1, 8),
-        memory.reshape(16, 128, 128),
-        normalizer.reshape(16, 128),
-        stabilizer,
+        partials, small, memory.reshape(16, 128, 128), normalizer.reshape(16, 128)
     )
     hidden = exchanged(hidden, ("kv_0", "tp"))
     spread = called(
@@ -336,7 +333,7 @@
     )(place, hidden.reshape(Z, 2048), tok, *w_all, w_other)
     spread = exchanged(spread, "kv_0").reshape(256, 256)
     spread = called(spread_kernel, shape((Y, 256, 256), bf16), flops=10**6)(spread)
-    spread = exchanged(spread, "kv_1")
+    spread = mirrored(spread)
     other = swapped(spread)
     keep, send, residual = called(
         mlp_kernel,
@@ -350,7 +347,7 @@
         scratch_shapes=[pltpu.VMEM((ROWS, D), bf16), pltpu.VMEM((ROWS, 256), bf16)],
     )(place, spread, other, gain_mlp.reshape(Z, 256), w_gate.T, w_up.T, w_down)
     terms = (keep + swapped(send).astype(f32)).astype(bf16)
-    terms = exchanged(terms, "kv_1").astype(f32).sum(axis=0).astype(bf16)
+    terms = mirrored(terms).astype(f32).sum(axis=0).astype(bf16)
     terms = exchanged(terms.reshape(Z, HALF, ROWS), "kv_0")
     mixed = called(finish_kernel, shape((HALF, ROWS), bf16), flops=10**6)(terms, residual)
     return (

time: 155 us -> 153 us (0.987)
  the two profiles are of different devices: /device:TPU:1 before, /device:TPU:2 now
where the time goes in v1:
time: 153 us; the launch traced here: 152 us
  blocking collectives  74.9 us (49%)
  starting transfers between devices  42 us (27%)
  waiting for transfers between devices  24 us (16%)
  Pallas kernels  9.73 us (6%)
    all_to_all x3, blocking collectives, exchanged(): return lax.all_to_all(x, axis, split_axis=0, concat_axis=0, tiled=True)  52.2 us
    all_to_all x2, starting transfers between devices, exchanged(): return lax.all_to_all(x, axis, split_axis=0, concat_axis=0, tiled=True)  27.7 us
    all_to_all x2, blocking collectives, mirrored(): lax.all_to_all(x, ('kv_1', 'tp'), split_axis=0, concat_axis=0, tiled=True...  22.6 us
    all_to_all x2, waiting for transfers between devices, exchanged(): return lax.all_to_all(x, axis, split_axis=0, concat_axis=0, tiled=True)  14.3 us
    ppermute x3, starting transfers between devices, layer(): lax.ppermute(w_own, 'kv_1', [(i, (i + step) % Y) for i in range(Y)])  8.37 us
    ppermute x3, waiting for transfers between devices, layer(): lax.ppermute(w_own, 'kv_1', [(i, (i + step) % Y) for i in range(Y)])  6.14 us
    ppermute x3, starting transfers between devices, swapped(): return lax.ppermute(x, 'tp', [(0, 1), (1, 0)])  5.87 us
    ppermute x3, waiting for transfers between devices, swapped(): return lax.ppermute(x, 'tp', [(0, 1), (1, 0)])  3.61 us
  transfers between devices with their start and end apart: 8, of which 5 were waited for; matrix products, arithmetic and copies ran while one was open for 0% of the time, Pallas kernels for 2%

profile of v1, /device:TPU:2, one launch (start us, length us, event | category | flops | bytes accessed | tf_op | source)
XLA Modules:
  0.0 151.9 jit_solution(4924140422880522860)
XLA Ops:
  0.6 2.6 %shard_map.192 = bf16[4,32,3328]{2,1,0:T(8,128)(2,1)} custom-call(bf16[64,128]{1,0:T(8,128)(2,1)} %bitcast.39, f32[1,64]{1,0:T(1,128)} %bitcast.43, bf16[8,64]{1,0:T(8,128)(2,1)} %bitcast.41, bf16[8,64]{1,0:T(8,128)(2,1)} %bitcast.42, bf16[64,1024]{1,0:T(8,128)(2,1)} %wq_ref.1, bf16[64,1024]{1,0:T(8,128)(2,1)} %wk_ref.1, bf16[64,1024]{1,0:T(8,128)(2,1)} %wv_ref.1), custom_call_target="tpu_custom_call" | custom-call | flops 52428800 | bytes 1000000 | tf_op jit(solution)/shard_map/pallas_call | solution.py:294
  3.2 17.5 %all_to_all.35.in_ref = bf16[4,32,3328]{2,1,0:T(8,128)(2,1)S(1)} all-to-all(bf16[4,32,3328]{2,1,0:T(8,128)(2,1)} %shard_map.192), channel_id=1, replica_groups=mesh['dp'=4,'kv_0'=16,'kv_1'=4,'tp'=2] {'kv_1'}, dimensions={0} | all-to-all | bytes 1703936 | tf_op jit(solution)/shard_map/all_to_all | solution.py:24
  20.7 0.0 copy-start
  20.7 0.8 shard_map.193
  21.5 15.3 %all-to-all-start.1 = ((bf16[16,2,3200]{2,1,0:T(2,128)(2,1)}), bf16[16,2,3200]{2,1,0:T(2,128)(2,1)S(1)}, u32[]{:S(2)}, u32[]{:S(2)}) async-start(bf16[16,2,3200]{2,1,0:T(2,128)(2,1)} %get-tuple-element.13), calls=%async_computation.1 | async-start | bytes 409600 | tf_op jit(solution)/shard_map/all_to_all | solution.py:24
  36.8 0.0 copy-done.4
  36.8 3.1 %collective-permute-start.2 = (bf16[64,1024]{1,0:T(8,128)(2,1)S(1)}, bf16[64,1024]{1,0:T(8,128)(2,1)S(1)}, u32[]{:S(2)}, u32[]{:S(2)}) collective-permute-start(bf16[64,1024]{1,0:T(8,128)(2,1)S(1)} %bitcast.29), channel_id=1, source_target_pairs={{0,6},{2,0},{4,2},{6,4},{1,7},{3,1},{5,3},{7,5},{8,14},{10,8},{12,... | collective-permute-start | bytes 393224 | tf_op jit(solution)/shard_map/ppermute | solution.py:308
  39.9 3.4 %collective-permute-start.1 = (bf16[64,1024]{1,0:T(8,128)(2,1)S(1)}, bf16[64,1024]{1,0:T(8,128)(2,1)S(1)}, u32[]{:S(2)}, u32[]{:S(2)}) collective-permute-start(bf16[64,1024]{1,0:T(8,128)(2,1)S(1)} %bitcast.30), channel_id=1, source_target_pairs={{0,4},{2,6},{4,0},{6,2},{1,5},{3,7},{5,1},{7,3},{8,12},{10,14},{12... | collective-permute-start | bytes 393224 | tf_op jit(solution)/shard_map/ppermute | solution.py:308
  43.3 1.9 %collective-permute-start = (bf16[64,1024]{1,0:T(8,128)(2,1)S(1)}, bf16[64,1024]{1,0:T(8,128)(2,1)S(1)}, u32[]{:S(2)}, u32[]{:S(2)}) collective-permute-start(bf16[64,1024]{1,0:T(8,128)(2,1)S(1)} %bitcast.31), channel_id=1, source_target_pairs={{0,2},{2,4},{4,6},{6,0},{1,3},{3,5},{5,7},{7,1},{8,10},{10,12},{12... | collective-permute-start | bytes 393224 | tf_op jit(solution)/shard_map/ppermute | solution.py:308
  45.2 0.0 collective-permute-done.2.w3_ref
  45.2 4.4 %collective-permute-done.1.w2_ref = bf16[64,1024]{1,0:T(8,128)(2,1)S(1)} collective-permute-done((bf16[64,1024]{1,0:T(8,128)(2,1)S(1)}, bf16[64,1024]{1,0:T(8,128)(2,1)S(1)}, u32[]{:S(2)}, u32[]{:S(2)}) %collective-permute-start.1) | collective-permute-done | bytes 131104 | tf_op jit(solution)/shard_map/ppermute | solution.py:308
  49.7 1.7 %collective-permute-done.w1_ref = bf16[64,1024]{1,0:T(8,128)(2,1)S(1)} collective-permute-done((bf16[64,1024]{1,0:T(8,128)(2,1)S(1)}, bf16[64,1024]{1,0:T(8,128)(2,1)S(1)}, u32[]{:S(2)}, u32[]{:S(2)}) %collective-permute-start) | collective-permute-done | bytes 131104 | tf_op jit(solution)/shard_map/ppermute | solution.py:308
  51.4 0.0 copy-start.7
  51.4 0.0 copy-start.8
  51.4 0.0 copy-start.9
  51.4 0.1 pad_maximum_fusion
  51.5 0.0 copy-start.5
  51.5 1.9 %collective-permute-start.3 = (bf16[4,64,1024]{2,1,0:T(8,128)(2,1)S(1)}, bf16[4,64,1024]{2,1,0:T(8,128)(2,1)S(1)}, u32[]{:S(2)}, u32[]{:S(2)}) collective-permute-start(bf16[4,64,1024]{2,1,0:T(8,128)(2,1)S(1)} %pad_maximum_fusion), channel_id=1, source_target_pairs={{0,1},{1,0},{2,3},{3,2},{4,5},{5,4},{6,7},{7,6},{8,9},{9,8},{10,11... | collective-permute-start | bytes 1572872 | tf_op jit(solution)/shard_map/ppermute | solution.py:35
  53.4 0.0 copy-done.7
  53.4 0.0 copy-done.8
  53.4 0.0 copy-done.9
  53.4 0.0 all-to-all-done.1.in_ref
  53.5 0.0 copy-done
  53.5 0.0 copy-done.5
  53.5 2.6 %shard_map.194 = (bf16[32,8,128]{2,1,0:T(8,128)(2,1)}, f32[16,128,128]{2,1,0:T(8,128)}, f32[16,128]{1,0:T(8,128)}, f32[2,8]{1,0:T(2,128)}) custom-call(bf16[16,2,3200]{2,1,0:T(2,128)(2,1)S(1)} %all-to-all-done.1.in_ref, f32[4,8]{1,0:T(4,128)S(1)} %pad_maximum_fusion.1.small_ref, f32[16,128,128]{2,1,0:T(8,128)S(1)} %bitcast.25, f32[16,128]{1,0:T(8,128)S(1)} %bitcast.37), custom_call_target="tpu_custom_call" | custom-call | flops 10000000 | bytes 1000000 | tf_op jit(solution)/shard_map/pallas_call | solution.py:313
  56.1 12.4 %all-to-all-start.2 = ((bf16[32,8,128]{2,1,0:T(8,128)(2,1)}), bf16[32,8,128]{2,1,0:T(8,128)(2,1)S(1)}, u32[]{:S(2)}, u32[]{:S(2)}) async-start(bf16[32,8,128]{2,1,0:T(8,128)(2,1)} %get-tuple-element.14), calls=%async_computation.2 | async-start | bytes 131072 | tf_op jit(solution)/shard_map/all_to_all | solution.py:24
  68.5 0.1 pad_add_fusion.place_ref
  68.6 14.3 %all-to-all-done.2 = bf16[32,8,128]{2,1,0:T(8,128)(2,1)S(1)} async-done(((bf16[32,8,128]{2,1,0:T(8,128)(2,1)}), bf16[32,8,128]{2,1,0:T(8,128)(2,1)S(1)}, u32[]{:S(2)}, u32[]{:S(2)}) %all-to-all-start.2) | async-done | bytes 65568 | tf_op jit(solution)/shard_map/all_to_all | solution.py:24
  82.9 0.0 collective-permute-done.3.other_ref
  82.9 0.0 copy-start.3
  83.0 1.0 shard_map.195
  84.0 16.7 %all_to_all.36 = bf16[16,16,256]{2,1,0:T(8,128)(2,1)S(1)} all-to-all(bf16[16,16,256]{2,1,0:T(8,128)(2,1)S(1)} %shard_map.195), channel_id=1, replica_groups=mesh['dp'=4,'kv_0'=16,'kv_1'=4,'tp'=2] {'kv_0'}, dimensions={0} | all-to-all | bytes 262144 | tf_op jit(solution)/shard_map/all_to_all | solution.py:24
  100.7 0.0 copy-start.6
  100.7 10.6 %all_to_all.37.own_ref = bf16[4,256,256]{2,1,0:T(8,128)(2,1)S(1)} all-to-all(bf16[4,256,256]{2,1,0:T(8,128)(2,1)S(1)} %shard_map.196), channel_id=1, replica_groups={{0,2,4,6},{7,5,3,1},{8,10,12,14},{15,13,11,9},{16,18,20,22},{23,21,19,1..., dimensions={0} | all-to-all | bytes 1048576 | tf_op jit(solution)/shard_map/all_to_all | solution.py:29
  111.4 1.9 %collective-permute-start.4 = (bf16[4,256,256]{2,1,0:T(8,128)(2,1)S(1)}, bf16[4,256,256]{2,1,0:T(8,128)(2,1)S(1)}, u32[]{:S(2)}, u32[]{:S(2)}) collective-permute-start(bf16[4,256,256]{2,1,0:T(8,128)(2,1)S(1)} %all_to_all.37.own_ref), channel_id=1, source_target_pairs={{0,1},{1,0},{2,3},{3,2},{4,5},{5,4},{6,7},{7,6},{8,9},{9,8},{10,11... | collective-permute-start | bytes 1572872 | tf_op jit(solution)/shard_map/ppermute | solution.py:35
  113.3 0.0 copy-done.6
  113.3 1.9 %collective-permute-done.4.other_ref = bf16[4,256,256]{2,1,0:T(8,128)(2,1)S(1)} collective-permute-done((bf16[4,256,256]{2,1,0:T(8,128)(2,1)S(1)}, bf16[4,256,256]{2,1,0:T(8,128)(2,1)S(1)}, u32[]{:S(2)}, u32[]{:S(2)}) %collective-permute-start.4) | collective-permute-done | bytes 524320 | tf_op jit(solution)/shard_map/ppermute | solution.py:35
  115.1 0.0 copy-done.3
  115.1 0.0 copy-done.1
  115.2 0.0 copy-done.2
  115.2 1.9 %shard_map.197 = (f32[4,512,128]{2,1,0:T(8,128)S(1)}, bf16[4,512,128]{2,1,0:T(8,128)(2,1)S(1)}, bf16[32,128]{1,0:T(8,128)(2,1)S(1)}) custom-call(s32[4]{0:T(128)S(1)} %pad_add_fusion.place_ref, bf16[4,256,256]{2,1,0:T(8,128)(2,1)S(1)} %all_to_all.37.own_ref, bf16[4,256,256]{2,1,0:T(8,128)(2,1)S(1)} %collective-permute-done.4.other_ref, ...), custom_call_target="tpu_custom_call" | custom-call | flops 276824064 | bytes 1000000 | tf_op jit(solution)/shard_map/pallas_call | solution.py:338
  117.0 2.0 %collective-permute-start.5 = (bf16[4,512,128]{2,1,0:T(8,128)(2,1)S(1)}, bf16[4,512,128]{2,1,0:T(8,128)(2,1)S(1)}, u32[]{:S(2)}, u32[]{:S(2)}) collective-permute-start(bf16[4,512,128]{2,1,0:T(8,128)(2,1)S(1)} %get-tuple-element.17), channel_id=1, source_target_pairs={{0,1},{1,0},{2,3},{3,2},{4,5},{5,4},{6,7},{7,6},{8,9},{9,8},{10,11... | collective-permute-start | bytes 1572872 | tf_op jit(solution)/shard_map/ppermute | solution.py:35
  119.1 1.8 %collective-permute-done.5 = bf16[4,512,128]{2,1,0:T(8,128)(2,1)S(1)} collective-permute-done((bf16[4,512,128]{2,1,0:T(8,128)(2,1)S(1)}, bf16[4,512,128]{2,1,0:T(8,128)(2,1)S(1)}, u32[]{:S(2)}, u32[]{:S(2)}) %collective-permute-start.5) | collective-permute-done | bytes 524320 | tf_op jit(solution)/shard_map/ppermute | solution.py:35
  120.8 0.1 add_convert_fusion
  121.0 12.0 %all_to_all.38 = bf16[4,512,128]{2,1,0:T(8,128)(2,1)S(1)} all-to-all(bf16[4,512,128]{2,1,0:T(8,128)(2,1)S(1)} %add_convert_fusion), channel_id=1, replica_groups={{0,2,4,6},{7,5,3,1},{8,10,12,14},{15,13,11,9},{16,18,20,22},{23,21,19,1..., dimensions={0} | all-to-all | bytes 1048576 | tf_op jit(solution)/shard_map/all_to_all | solution.py:29
  133.0 0.1 reduce_sum.12
  133.1 18.1 %all_to_all.39.in_ref = bf16[16,32,128]{2,1,0:T(8,128)(2,1)S(1)} all-to-all(bf16[16,32,128]{2,1,0:T(8,128)(2,1)S(1)} %bitcast.38), channel_id=1, replica_groups=mesh['dp'=4,'kv_0'=16,'kv_1'=4,'tp'=2] {'kv_0'}, dimensions={0} | all-to-all | bytes 262144 | tf_op jit(solution)/shard_map/all_to_all | solution.py:24
  151.2 0.8 shard_map.198
  (7 shorter events, 0.1 us)
Async XLA Ops:
  20.7 32.8 %copy-start = (f32[2,8,128,128]{3,2,1,0:T(8,128)S(1)}, f32[2,8,128,128]{3,2,1,0:T(8,128)}, u32[]{:S(2)}) copy-start(f32[2,8,128,128]{3,2,1,0:T(8,128)} %param.26) | copy-start | bytes 3145732
  21.5 15.3 %copy-start.4 = (bf16[1024,64]{0,1:T(8,128)(2,1)S(1)}, bf16[1024,64]{0,1:T(8,128)(2,1)}, u32[]{:S(2)}) copy-start(bf16[1024,64]{0,1:T(8,128)(2,1)} %param.29) | copy-start | bytes 393220
  21.5 32.0 %all-to-all-start.1 = ((bf16[16,2,3200]{2,1,0:T(2,128)(2,1)}), bf16[16,2,3200]{2,1,0:T(2,128)(2,1)S(1)}, u32[]{:S(2)}, u32[]{:S(2)}) async-start(bf16[16,2,3200]{2,1,0:T(2,128)(2,1)} %get-tuple-element.13), calls=%async_computation.1 | async-start | bytes 409600 | tf_op jit(solution)/shard_map/all_to_all | solution.py:24
  36.8 8.4 %collective-permute-start.2 = (bf16[64,1024]{1,0:T(8,128)(2,1)S(1)}, bf16[64,1024]{1,0:T(8,128)(2,1)S(1)}, u32[]{:S(2)}, u32[]{:S(2)}) collective-permute-start(bf16[64,1024]{1,0:T(8,128)(2,1)S(1)} %bitcast.29), channel_id=1, source_target_pairs={{0,6},{2,0},{4,2},{6,4},{1,7},{3,1},{5,3},{7,5},{8,14},{10,8},{12,... | collective-permute-start | bytes 393224 | tf_op jit(solution)/shard_map/ppermute | solution.py:308
  39.9 9.7 %collective-permute-start.1 = (bf16[64,1024]{1,0:T(8,128)(2,1)S(1)}, bf16[64,1024]{1,0:T(8,128)(2,1)S(1)}, u32[]{:S(2)}, u32[]{:S(2)}) collective-permute-start(bf16[64,1024]{1,0:T(8,128)(2,1)S(1)} %bitcast.30), channel_id=1, source_target_pairs={{0,4},{2,6},{4,0},{6,2},{1,5},{3,7},{5,1},{7,3},{8,12},{10,14},{12... | collective-permute-start | bytes 393224 | tf_op jit(solution)/shard_map/ppermute | solution.py:308
  43.3 8.1 %collective-permute-start = (bf16[64,1024]{1,0:T(8,128)(2,1)S(1)}, bf16[64,1024]{1,0:T(8,128)(2,1)S(1)}, u32[]{:S(2)}, u32[]{:S(2)}) collective-permute-start(bf16[64,1024]{1,0:T(8,128)(2,1)S(1)} %bitcast.31), channel_id=1, source_target_pairs={{0,2},{2,4},{4,6},{6,0},{1,3},{3,5},{5,7},{7,1},{8,10},{10,12},{12... | collective-permute-start | bytes 393224 | tf_op jit(solution)/shard_map/ppermute | solution.py:308
  51.4 2.0 %copy-start.7 = (f32[2,8]{1,0:T(2,128)S(1)}, f32[2,8]{1,0:T(2,128)}, u32[]{:S(2)}) copy-start(f32[2,8]{1,0:T(2,128)} %param.28) | copy-start | bytes 196
  51.4 2.0 %copy-start.8 = (f32[8]{0:T(128)S(1)}, f32[8]{0:T(128)}, u32[]{:S(2)}) copy-start(f32[8]{0:T(128)} %param.25) | copy-start | bytes 100
  51.4 2.0 %copy-start.9 = (f32[8]{0:T(128)S(1)}, f32[8]{0:T(128)}, u32[]{:S(2)}) copy-start(f32[8]{0:T(128)} %param.24) | copy-start | bytes 100
  51.5 2.0 %copy-start.5 = (f32[2,8,128]{2,1,0:T(8,128)S(1)}, f32[2,8,128]{2,1,0:T(8,128)}, u32[]{:S(2)}) copy-start(f32[2,8,128]{2,1,0:T(8,128)} %param.27) | copy-start | bytes 24580
  51.5 31.5 %collective-permute-start.3 = (bf16[4,64,1024]{2,1,0:T(8,128)(2,1)S(1)}, bf16[4,64,1024]{2,1,0:T(8,128)(2,1)S(1)}, u32[]{:S(2)}, u32[]{:S(2)}) collective-permute-start(bf16[4,64,1024]{2,1,0:T(8,128)(2,1)S(1)} %pad_maximum_fusion), channel_id=1, source_target_pairs={{0,1},{1,0},{2,3},{3,2},{4,5},{5,4},{6,7},{7,6},{8,9},{9,8},{10,11... | collective-permute-start | bytes 1572872 | tf_op jit(solution)/shard_map/ppermute | solution.py:35
  56.1 26.8 %all-to-all-start.2 = ((bf16[32,8,128]{2,1,0:T(8,128)(2,1)}), bf16[32,8,128]{2,1,0:T(8,128)(2,1)S(1)}, u32[]{:S(2)}, u32[]{:S(2)}) async-start(bf16[32,8,128]{2,1,0:T(8,128)(2,1)} %get-tuple-element.14), calls=%async_computation.2 | async-start | bytes 131072 | tf_op jit(solution)/shard_map/all_to_all | solution.py:24
  82.9 32.2 %copy-start.3 = (bf16[88,4096]{1,0:T(8,128)(2,1)S(1)}, bf16[88,4096]{1,0:T(8,128)(2,1)}, u32[]{:S(2)}) copy-start(bf16[88,4096]{1,0:T(8,128)(2,1)} %wd_ref.1) | copy-start | bytes 2162692
  100.7 14.5 %copy-start.1 = (bf16[4096,88]{0,1:T(8,128)(2,1)S(1)}, bf16[4096,88]{0,1:T(8,128)(2,1)}, u32[]{:S(2)}) copy-start(bf16[4096,88]{0,1:T(8,128)(2,1)} %param.31) | copy-start | bytes 2162692
  100.7 14.5 %copy-start.2 = (bf16[4096,88]{0,1:T(8,128)(2,1)S(1)}, bf16[4096,88]{0,1:T(8,128)(2,1)}, u32[]{:S(2)}) copy-start(bf16[4096,88]{0,1:T(8,128)(2,1)} %param.32) | copy-start | bytes 2162692
  100.7 12.5 %copy-start.6 = (f32[4096]{0:T(1024)S(1)}, f32[4096]{0:T(1024)}, u32[]{:S(2)}) copy-start(f32[4096]{0:T(1024)} %param.30) | copy-start | bytes 49156
  111.4 3.8 %collective-permute-start.4 = (bf16[4,256,256]{2,1,0:T(8,128)(2,1)S(1)}, bf16[4,256,256]{2,1,0:T(8,128)(2,1)S(1)}, u32[]{:S(2)}, u32[]{:S(2)}) collective-permute-start(bf16[4,256,256]{2,1,0:T(8,128)(2,1)S(1)} %all_to_all.37.own_ref), channel_id=1, source_target_pairs={{0,1},{1,0},{2,3},{3,2},{4,5},{5,4},{6,7},{7,6},{8,9},{9,8},{10,11... | collective-permute-start | bytes 1572872 | tf_op jit(solution)/shard_map/ppermute | solution.py:35
  117.0 3.8 %collective-permute-start.5 = (bf16[4,512,128]{2,1,0:T(8,128)(2,1)S(1)}, bf16[4,512,128]{2,1,0:T(8,128)(2,1)S(1)}, u32[]{:S(2)}, u32[]{:S(2)}) collective-permute-start(bf16[4,512,128]{2,1,0:T(8,128)(2,1)S(1)} %get-tuple-element.17), channel_id=1, source_target_pairs={{0,1},{1,0},{2,3},{3,2},{4,5},{5,4},{6,7},{7,6},{8,9},{9,8},{10,11... | collective-permute-start | bytes 1572872 | tf_op jit(solution)/shard_map/ppermute | solution.py:35

commit v2 on v1

--- a/solution.py
+++ b/solution.py
@@ -25,7 +25,7 @@
 
 
 def mirrored(x):
-    groups = [[0, 2, 4, 6], [7, 5, 3, 1]]
+    groups = [[0, 2, 4, 6], [5, 7, 1, 3]]
     return lax.all_to_all(
         x, ("kv_1", "tp"), split_axis=0, concat_axis=0, tiled=True, axis_index_groups=groups
     )
@@ -203,8 +203,8 @@
     keep_ref, send_ref, res_ref, x_ref, block_ref,
 ):
     first = place_ref[0] == 0
-    mine = [jnp.where(first, y, Y - 1 - y) for y in range(Y)]
-    theirs = [jnp.where(first, Y - 1 - y, y) for y in range(Y)]
+    mine = [jnp.where(first, y, (y + 2) % Y) for y in range(Y)]
+    theirs = [jnp.where(first, (y + 2) % Y, y) for y in range(Y)]
     squares = [jnp.zeros((Z, 256), f32) for _ in range(2 * Y)]
     for z in range(Z):
         gain = gain_ref[z : z + 1, :]

time: 153 us -> 152 us (level)
  the two profiles are of different devices: /device:TPU:2 before, /device:TPU:14 now
where the time goes in v2:
time: 152 us
  blocking collectives  76.2 us (50%)
  starting transfers between devices  42.5 us (28%)
  waiting for transfers between devices  21.8 us (14%)
  Pallas kernels  9.72 us (6%)
    all_to_all x3, blocking collectives, exchanged(): return lax.all_to_all(x, axis, split_axis=0, concat_axis=0, tiled=True)  52.2 us
    all_to_all x2, starting transfers between devices, exchanged(): return lax.all_to_all(x, axis, split_axis=0, concat_axis=0, tiled=True)  26.8 us
    all_to_all x2, blocking collectives, mirrored(): lax.all_to_all(x, ('kv_1', 'tp'), split_axis=0, concat_axis=0, tiled=True...  24.1 us
    all_to_all x2, waiting for transfers between devices, exchanged(): return lax.all_to_all(x, axis, split_axis=0, concat_axis=0, tiled=True)  15.3 us
    ppermute x3, starting transfers between devices, layer(): lax.ppermute(w_own, 'kv_1', [(i, (i + step) % Y) for i in range(Y)])  9.82 us
    ppermute x3, starting transfers between devices, swapped(): return lax.ppermute(x, 'tp', [(0, 1), (1, 0)])  5.87 us
    ppermute x3, waiting for transfers between devices, swapped(): return lax.ppermute(x, 'tp', [(0, 1), (1, 0)])  3.61 us
  transfers between devices with their start and end apart: 8, of which 6 were waited for; matrix products, arithmetic and copies ran while one was open for 0% of the time, Pallas kernels for 2%

profile of v2, /device:TPU:14, one launch (start us, length us, event | category | flops | bytes accessed | tf_op | source)
XLA Modules:
  0.0 151.5 jit_solution(18302562202297233492)
XLA Ops:
  0.6 2.6 %shard_map.192 = bf16[4,32,3328]{2,1,0:T(8,128)(2,1)} custom-call(bf16[64,128]{1,0:T(8,128)(2,1)} %bitcast.39, f32[1,64]{1,0:T(1,128)} %bitcast.43, bf16[8,64]{1,0:T(8,128)(2,1)} %bitcast.41, bf16[8,64]{1,0:T(8,128)(2,1)} %bitcast.42, bf16[64,1024]{1,0:T(8,128)(2,1)} %wq_ref.1, bf16[64,1024]{1,0:T(8,128)(2,1)} %wk_ref.1, bf16[64,1024]{1,0:T(8,128)(2,1)} %wv_ref.1), custom_call_target="tpu_custom_call" | custom-call | flops 52428800 | bytes 1000000 | tf_op jit(solution)/shard_map/pallas_call | solution.py:294
  3.2 16.4 %all_to_all.35.in_ref = bf16[4,32,3328]{2,1,0:T(8,128)(2,1)S(1)} all-to-all(bf16[4,32,3328]{2,1,0:T(8,128)(2,1)} %shard_map.192), channel_id=1, replica_groups=mesh['dp'=4,'kv_0'=16,'kv_1'=4,'tp'=2] {'kv_1'}, dimensions={0} | all-to-all | bytes 1703936 | tf_op jit(solution)/shard_map/all_to_all | solution.py:24
  19.6 0.0 copy-start
  19.6 0.8 shard_map.193
  20.5 0.0 copy-start.4
  20.5 15.3 %all-to-all-start.1 = ((bf16[16,2,3200]{2,1,0:T(2,128)(2,1)}), bf16[16,2,3200]{2,1,0:T(2,128)(2,1)S(1)}, u32[]{:S(2)}, u32[]{:S(2)}) async-start(bf16[16,2,3200]{2,1,0:T(2,128)(2,1)} %get-tuple-element.13), calls=%async_computation.1 | async-start | bytes 409600 | tf_op jit(solution)/shard_map/all_to_all | solution.py:24
  35.8 0.0 copy-done.4
  35.8 3.4 %collective-permute-start.2 = (bf16[64,1024]{1,0:T(8,128)(2,1)S(1)}, bf16[64,1024]{1,0:T(8,128)(2,1)S(1)}, u32[]{:S(2)}, u32[]{:S(2)}) collective-permute-start(bf16[64,1024]{1,0:T(8,128)(2,1)S(1)} %bitcast.29), channel_id=1, source_target_pairs={{0,6},{2,0},{4,2},{6,4},{1,7},{3,1},{5,3},{7,5},{8,14},{10,8},{12,... | collective-permute-start | bytes 393224 | tf_op jit(solution)/shard_map/ppermute | solution.py:308
  39.2 2.3 %collective-permute-start.1 = (bf16[64,1024]{1,0:T(8,128)(2,1)S(1)}, bf16[64,1024]{1,0:T(8,128)(2,1)S(1)}, u32[]{:S(2)}, u32[]{:S(2)}) collective-permute-start(bf16[64,1024]{1,0:T(8,128)(2,1)S(1)} %bitcast.30), channel_id=1, source_target_pairs={{0,4},{2,6},{4,0},{6,2},{1,5},{3,7},{5,1},{7,3},{8,12},{10,14},{12... | collective-permute-start | bytes 393224 | tf_op jit(solution)/shard_map/ppermute | solution.py:308
  41.5 4.2 %collective-permute-start = (bf16[64,1024]{1,0:T(8,128)(2,1)S(1)}, bf16[64,1024]{1,0:T(8,128)(2,1)S(1)}, u32[]{:S(2)}, u32[]{:S(2)}) collective-permute-start(bf16[64,1024]{1,0:T(8,128)(2,1)S(1)} %bitcast.31), channel_id=1, source_target_pairs={{0,2},{2,4},{4,6},{6,0},{1,3},{3,5},{5,7},{7,1},{8,10},{10,12},{12... | collective-permute-start | bytes 393224 | tf_op jit(solution)/shard_map/ppermute | solution.py:308
  45.7 0.0 collective-permute-done.2.w3_ref
  45.7 1.9 %collective-permute-done.1.w2_ref = bf16[64,1024]{1,0:T(8,128)(2,1)S(1)} collective-permute-done((bf16[64,1024]{1,0:T(8,128)(2,1)S(1)}, bf16[64,1024]{1,0:T(8,128)(2,1)S(1)}, u32[]{:S(2)}, u32[]{:S(2)}) %collective-permute-start.1) | collective-permute-done | bytes 131104 | tf_op jit(solution)/shard_map/ppermute | solution.py:308
  47.6 1.0 collective-permute-done.w1_ref
  48.6 0.0 copy-start.7
  48.6 0.0 copy-start.8
  48.6 0.1 pad_maximum_fusion
  48.7 0.0 copy-start.5
  48.7 1.9 %collective-permute-start.3 = (bf16[4,64,1024]{2,1,0:T(8,128)(2,1)S(1)}, bf16[4,64,1024]{2,1,0:T(8,128)(2,1)S(1)}, u32[]{:S(2)}, u32[]{:S(2)}) collective-permute-start(bf16[4,64,1024]{2,1,0:T(8,128)(2,1)S(1)} %pad_maximum_fusion), channel_id=1, source_target_pairs={{0,1},{1,0},{2,3},{3,2},{4,5},{5,4},{6,7},{7,6},{8,9},{9,8},{10,11... | collective-permute-start | bytes 1572872 | tf_op jit(solution)/shard_map/ppermute | solution.py:35
  50.6 0.0 copy-done.7
  50.6 0.0 copy-done.8
  50.6 0.0 copy-done.9
  50.7 1.0 all-to-all-done.1.in_ref
  51.7 0.0 copy-done
  51.7 0.0 copy-done.5
  51.7 2.6 %shard_map.194 = (bf16[32,8,128]{2,1,0:T(8,128)(2,1)}, f32[16,128,128]{2,1,0:T(8,128)}, f32[16,128]{1,0:T(8,128)}, f32[2,8]{1,0:T(2,128)}) custom-call(bf16[16,2,3200]{2,1,0:T(2,128)(2,1)S(1)} %all-to-all-done.1.in_ref, f32[4,8]{1,0:T(4,128)S(1)} %pad_maximum_fusion.1.small_ref, f32[16,128,128]{2,1,0:T(8,128)S(1)} %bitcast.25, f32[16,128]{1,0:T(8,128)S(1)} %bitcast.37), custom_call_target="tpu_custom_call" | custom-call | flops 10000000 | bytes 1000000 | tf_op jit(solution)/shard_map/pallas_call | solution.py:313
  54.3 11.4 %all-to-all-start.2 = ((bf16[32,8,128]{2,1,0:T(8,128)(2,1)}), bf16[32,8,128]{2,1,0:T(8,128)(2,1)S(1)}, u32[]{:S(2)}, u32[]{:S(2)}) async-start(bf16[32,8,128]{2,1,0:T(8,128)(2,1)} %get-tuple-element.14), calls=%async_computation.2 | async-start | bytes 131072 | tf_op jit(solution)/shard_map/all_to_all | solution.py:24
  65.8 0.1 pad_add_fusion.place_ref
  65.8 14.3 %all-to-all-done.2 = bf16[32,8,128]{2,1,0:T(8,128)(2,1)S(1)} async-done(((bf16[32,8,128]{2,1,0:T(8,128)(2,1)}), bf16[32,8,128]{2,1,0:T(8,128)(2,1)S(1)}, u32[]{:S(2)}, u32[]{:S(2)}) %all-to-all-start.2) | async-done | bytes 65568 | tf_op jit(solution)/shard_map/all_to_all | solution.py:24
  80.2 0.0 collective-permute-done.3.other_ref
  80.2 0.0 copy-start.3
  80.2 1.0 shard_map.195
  81.2 16.7 %all_to_all.36 = bf16[16,16,256]{2,1,0:T(8,128)(2,1)S(1)} all-to-all(bf16[16,16,256]{2,1,0:T(8,128)(2,1)S(1)} %shard_map.195), channel_id=1, replica_groups=mesh['dp'=4,'kv_0'=16,'kv_1'=4,'tp'=2] {'kv_0'}, dimensions={0} | all-to-all | bytes 262144 | tf_op jit(solution)/shard_map/all_to_all | solution.py:24
  97.9 0.0 copy-start.6
  98.0 12.4 %all_to_all.37.own_ref = bf16[4,256,256]{2,1,0:T(8,128)(2,1)S(1)} all-to-all(bf16[4,256,256]{2,1,0:T(8,128)(2,1)S(1)} %shard_map.196), channel_id=1, replica_groups={{0,2,4,6},{5,7,1,3},{8,10,12,14},{13,15,9,11},{16,18,20,22},{21,23,17,1..., dimensions={0} | all-to-all | bytes 1048576 | tf_op jit(solution)/shard_map/all_to_all | solution.py:29
  110.3 1.9 %collective-permute-start.4 = (bf16[4,256,256]{2,1,0:T(8,128)(2,1)S(1)}, bf16[4,256,256]{2,1,0:T(8,128)(2,1)S(1)}, u32[]{:S(2)}, u32[]{:S(2)}) collective-permute-start(bf16[4,256,256]{2,1,0:T(8,128)(2,1)S(1)} %all_to_all.37.own_ref), channel_id=1, source_target_pairs={{0,1},{1,0},{2,3},{3,2},{4,5},{5,4},{6,7},{7,6},{8,9},{9,8},{10,11... | collective-permute-start | bytes 1572872 | tf_op jit(solution)/shard_map/ppermute | solution.py:35
  112.3 0.0 copy-done.6
  112.3 1.9 %collective-permute-done.4.other_ref = bf16[4,256,256]{2,1,0:T(8,128)(2,1)S(1)} collective-permute-done((bf16[4,256,256]{2,1,0:T(8,128)(2,1)S(1)}, bf16[4,256,256]{2,1,0:T(8,128)(2,1)S(1)}, u32[]{:S(2)}, u32[]{:S(2)}) %collective-permute-start.4) | collective-permute-done | bytes 524320 | tf_op jit(solution)/shard_map/ppermute | solution.py:35
  114.1 0.0 copy-done.3
  114.1 0.0 copy-done.1
  114.1 0.0 copy-done.2
  114.1 1.9 %shard_map.197 = (f32[4,512,128]{2,1,0:T(8,128)S(1)}, bf16[4,512,128]{2,1,0:T(8,128)(2,1)S(1)}, bf16[32,128]{1,0:T(8,128)(2,1)S(1)}) custom-call(s32[4]{0:T(128)S(1)} %pad_add_fusion.place_ref, bf16[4,256,256]{2,1,0:T(8,128)(2,1)S(1)} %all_to_all.37.own_ref, bf16[4,256,256]{2,1,0:T(8,128)(2,1)S(1)} %collective-permute-done.4.other_ref, ...), custom_call_target="tpu_custom_call" | custom-call | flops 276824064 | bytes 1000000 | tf_op jit(solution)/shard_map/pallas_call | solution.py:338
  116.0 2.0 %collective-permute-start.5 = (bf16[4,512,128]{2,1,0:T(8,128)(2,1)S(1)}, bf16[4,512,128]{2,1,0:T(8,128)(2,1)S(1)}, u32[]{:S(2)}, u32[]{:S(2)}) collective-permute-start(bf16[4,512,128]{2,1,0:T(8,128)(2,1)S(1)} %get-tuple-element.17), channel_id=1, source_target_pairs={{0,1},{1,0},{2,3},{3,2},{4,5},{5,4},{6,7},{7,6},{8,9},{9,8},{10,11... | collective-permute-start | bytes 1572872 | tf_op jit(solution)/shard_map/ppermute | solution.py:35
  118.1 1.8 %collective-permute-done.5 = bf16[4,512,128]{2,1,0:T(8,128)(2,1)S(1)} collective-permute-done((bf16[4,512,128]{2,1,0:T(8,128)(2,1)S(1)}, bf16[4,512,128]{2,1,0:T(8,128)(2,1)S(1)}, u32[]{:S(2)}, u32[]{:S(2)}) %collective-permute-start.5) | collective-permute-done | bytes 524320 | tf_op jit(solution)/shard_map/ppermute | solution.py:35
  119.8 0.1 add_convert_fusion
  120.0 11.7 %all_to_all.38 = bf16[4,512,128]{2,1,0:T(8,128)(2,1)S(1)} all-to-all(bf16[4,512,128]{2,1,0:T(8,128)(2,1)S(1)} %add_convert_fusion), channel_id=1, replica_groups={{0,2,4,6},{5,7,1,3},{8,10,12,14},{13,15,9,11},{16,18,20,22},{21,23,17,1..., dimensions={0} | all-to-all | bytes 1048576 | tf_op jit(solution)/shard_map/all_to_all | solution.py:29
  131.7 0.1 reduce_sum.12
  131.7 19.0 %all_to_all.39.in_ref = bf16[16,32,128]{2,1,0:T(8,128)(2,1)S(1)} all-to-all(bf16[16,32,128]{2,1,0:T(8,128)(2,1)S(1)} %bitcast.38), channel_id=1, replica_groups=mesh['dp'=4,'kv_0'=16,'kv_1'=4,'tp'=2] {'kv_0'}, dimensions={0} | all-to-all | bytes 262144 | tf_op jit(solution)/shard_map/all_to_all | solution.py:24
  150.8 0.8 shard_map.198
  (7 shorter events, 0.1 us)
Async XLA Ops:
  19.6 32.0 %copy-start = (f32[2,8,128,128]{3,2,1,0:T(8,128)S(1)}, f32[2,8,128,128]{3,2,1,0:T(8,128)}, u32[]{:S(2)}) copy-start(f32[2,8,128,128]{3,2,1,0:T(8,128)} %param.26) | copy-start | bytes 3145732
  20.5 15.3 %copy-start.4 = (bf16[1024,64]{0,1:T(8,128)(2,1)S(1)}, bf16[1024,64]{0,1:T(8,128)(2,1)}, u32[]{:S(2)}) copy-start(bf16[1024,64]{0,1:T(8,128)(2,1)} %param.29) | copy-start | bytes 393220
  20.5 31.2 %all-to-all-start.1 = ((bf16[16,2,3200]{2,1,0:T(2,128)(2,1)}), bf16[16,2,3200]{2,1,0:T(2,128)(2,1)S(1)}, u32[]{:S(2)}, u32[]{:S(2)}) async-start(bf16[16,2,3200]{2,1,0:T(2,128)(2,1)} %get-tuple-element.13), calls=%async_computation.1 | async-start | bytes 409600 | tf_op jit(solution)/shard_map/all_to_all | solution.py:24
  35.8 9.8 %collective-permute-start.2 = (bf16[64,1024]{1,0:T(8,128)(2,1)S(1)}, bf16[64,1024]{1,0:T(8,128)(2,1)S(1)}, u32[]{:S(2)}, u32[]{:S(2)}) collective-permute-start(bf16[64,1024]{1,0:T(8,128)(2,1)S(1)} %bitcast.29), channel_id=1, source_target_pairs={{0,6},{2,0},{4,2},{6,4},{1,7},{3,1},{5,3},{7,5},{8,14},{10,8},{12,... | collective-permute-start | bytes 393224 | tf_op jit(solution)/shard_map/ppermute | solution.py:308
  39.2 8.4 %collective-permute-start.1 = (bf16[64,1024]{1,0:T(8,128)(2,1)S(1)}, bf16[64,1024]{1,0:T(8,128)(2,1)S(1)}, u32[]{:S(2)}, u32[]{:S(2)}) collective-permute-start(bf16[64,1024]{1,0:T(8,128)(2,1)S(1)} %bitcast.30), channel_id=1, source_target_pairs={{0,4},{2,6},{4,0},{6,2},{1,5},{3,7},{5,1},{7,3},{8,12},{10,14},{12... | collective-permute-start | bytes 393224 | tf_op jit(solution)/shard_map/ppermute | solution.py:308
  41.5 7.1 %collective-permute-start = (bf16[64,1024]{1,0:T(8,128)(2,1)S(1)}, bf16[64,1024]{1,0:T(8,128)(2,1)S(1)}, u32[]{:S(2)}, u32[]{:S(2)}) collective-permute-start(bf16[64,1024]{1,0:T(8,128)(2,1)S(1)} %bitcast.31), channel_id=1, source_target_pairs={{0,2},{2,4},{4,6},{6,0},{1,3},{3,5},{5,7},{7,1},{8,10},{10,12},{12... | collective-permute-start | bytes 393224 | tf_op jit(solution)/shard_map/ppermute | solution.py:308
  48.6 2.0 %copy-start.7 = (f32[2,8]{1,0:T(2,128)S(1)}, f32[2,8]{1,0:T(2,128)}, u32[]{:S(2)}) copy-start(f32[2,8]{1,0:T(2,128)} %param.28) | copy-start | bytes 196
  48.6 2.0 %copy-start.8 = (f32[8]{0:T(128)S(1)}, f32[8]{0:T(128)}, u32[]{:S(2)}) copy-start(f32[8]{0:T(128)} %param.25) | copy-start | bytes 100
  48.6 2.0 %copy-start.9 = (f32[8]{0:T(128)S(1)}, f32[8]{0:T(128)}, u32[]{:S(2)}) copy-start(f32[8]{0:T(128)} %param.24) | copy-start | bytes 100
  48.7 3.0 %copy-start.5 = (f32[2,8,128]{2,1,0:T(8,128)S(1)}, f32[2,8,128]{2,1,0:T(8,128)}, u32[]{:S(2)}) copy-start(f32[2,8,128]{2,1,0:T(8,128)} %param.27) | copy-start | bytes 24580
  48.7 31.5 %collective-permute-start.3 = (bf16[4,64,1024]{2,1,0:T(8,128)(2,1)S(1)}, bf16[4,64,1024]{2,1,0:T(8,128)(2,1)S(1)}, u32[]{:S(2)}, u32[]{:S(2)}) collective-permute-start(bf16[4,64,1024]{2,1,0:T(8,128)(2,1)S(1)} %pad_maximum_fusion), channel_id=1, source_target_pairs={{0,1},{1,0},{2,3},{3,2},{4,5},{5,4},{6,7},{7,6},{8,9},{9,8},{10,11... | collective-permute-start | bytes 1572872 | tf_op jit(solution)/shard_map/ppermute | solution.py:35
  54.3 25.8 %all-to-all-start.2 = ((bf16[32,8,128]{2,1,0:T(8,128)(2,1)}), bf16[32,8,128]{2,1,0:T(8,128)(2,1)S(1)}, u32[]{:S(2)}, u32[]{:S(2)}) async-start(bf16[32,8,128]{2,1,0:T(8,128)(2,1)} %get-tuple-element.14), calls=%async_computation.2 | async-start | bytes 131072 | tf_op jit(solution)/shard_map/all_to_all | solution.py:24
  80.2 34.0 %copy-start.3 = (bf16[88,4096]{1,0:T(8,128)(2,1)S(1)}, bf16[88,4096]{1,0:T(8,128)(2,1)}, u32[]{:S(2)}) copy-start(bf16[88,4096]{1,0:T(8,128)(2,1)} %wd_ref.1) | copy-start | bytes 2162692
  97.9 16.2 %copy-start.1 = (bf16[4096,88]{0,1:T(8,128)(2,1)S(1)}, bf16[4096,88]{0,1:T(8,128)(2,1)}, u32[]{:S(2)}) copy-start(bf16[4096,88]{0,1:T(8,128)(2,1)} %param.31) | copy-start | bytes 2162692
  97.9 16.2 %copy-start.2 = (bf16[4096,88]{0,1:T(8,128)(2,1)S(1)}, bf16[4096,88]{0,1:T(8,128)(2,1)}, u32[]{:S(2)}) copy-start(bf16[4096,88]{0,1:T(8,128)(2,1)} %param.32) | copy-start | bytes 2162692
  97.9 14.3 %copy-start.6 = (f32[4096]{0:T(1024)S(1)}, f32[4096]{0:T(1024)}, u32[]{:S(2)}) copy-start(f32[4096]{0:T(1024)} %param.30) | copy-start | bytes 49156
  110.3 3.8 %collective-permute-start.4 = (bf16[4,256,256]{2,1,0:T(8,128)(2,1)S(1)}, bf16[4,256,256]{2,1,0:T(8,128)(2,1)S(1)}, u32[]{:S(2)}, u32[]{:S(2)}) collective-permute-start(bf16[4,256,256]{2,1,0:T(8,128)(2,1)S(1)} %all_to_all.37.own_ref), channel_id=1, source_target_pairs={{0,1},{1,0},{2,3},{3,2},{4,5},{5,4},{6,7},{7,6},{8,9},{9,8},{10,11... | collective-permute-start | bytes 1572872 | tf_op jit(solution)/shard_map/ppermute | solution.py:35
  116.0 3.8 %collective-permute-start.5 = (bf16[4,512,128]{2,1,0:T(8,128)(2,1)S(1)}, bf16[4,512,128]{2,1,0:T(8,128)(2,1)S(1)}, u32[]{:S(2)}, u32[]{:S(2)}) collective-permute-start(bf16[4,512,128]{2,1,0:T(8,128)(2,1)S(1)} %get-tuple-element.17), channel_id=1, source_target_pairs={{0,1},{1,0},{2,3},{3,2},{4,5},{5,4},{6,7},{7,6},{8,9},{9,8},{10,11... | collective-permute-start | bytes 1572872 | tf_op jit(solution)/shard_map/ppermute | solution.py:35

commit v3 on v2

--- a/solution.py
+++ b/solution.py
@@ -209,8 +209,8 @@
     for z in range(Z):
         gain = gain_ref[z : z + 1, :]
         for y in range(Y):
-            own = own_ref[mine[y], Z * z : Z * (z + 1), :].astype(f32)
-            other = other_ref[theirs[y], Z * z : Z * (z + 1), :].astype(f32)
+            own = own_ref[y, Z * z : Z * (z + 1), :].astype(f32)
+            other = other_ref[y, Z * z : Z * (z + 1), :].astype(f32)
             for n, x in enumerate((jnp.where(first, own, other), jnp.where(first, other, own))):
                 at = Y * n + y
                 squares[at] = squares[at] + x * x
@@ -221,8 +221,8 @@
 
     here = pl.multiple_of(Z * place_ref[3], Z)
     for y in range(Y):
-        own = own_ref[mine[y], pl.ds(here, Z), :]
-        other = other_ref[theirs[y], pl.ds(here, Z), :]
+        own = own_ref[y, pl.ds(here, Z), :]
+        other = other_ref[y, pl.ds(here, Z), :]
         block_ref[Z * y : Z * (y + 1), :] = jnp.where(first, own, other)
         block_ref[64 + Z * y : 64 + Z * (y + 1), :] = jnp.where(first, other, own)
     at = lax.broadcasted_iota(jnp.int32, (HALF, 256), 0)
@@ -333,7 +333,7 @@
     )(place, hidden.reshape(Z, 2048), tok, *w_all, w_other)
     spread = exchanged(spread, "kv_0").reshape(256, 256)
     spread = called(spread_kernel, shape((Y, 256, 256), bf16), flops=10**6)(spread)
-    spread = mirrored(spread)
+    spread = exchanged(spread, "kv_1")
     other = swapped(spread)
     keep, send, residual = called(
         mlp_kernel,

time: 152 us -> 152 us (level)
  the two profiles are of different devices: /device:TPU:14 before, /device:TPU:6 now
where the time goes in v3:
time: 152 us; the launch traced here: 151 us
  blocking collectives  74.3 us (49%)
  starting transfers between devices  42 us (28%)
  waiting for transfers between devices  24 us (16%)
  Pallas kernels  9.72 us (6%)
    all_to_all x4, blocking collectives, exchanged(): return lax.all_to_all(x, axis, split_axis=0, concat_axis=0, tiled=True)  62.9 us
    all_to_all x2, starting transfers between devices, exchanged(): return lax.all_to_all(x, axis, split_axis=0, concat_axis=0, tiled=True)  27.7 us
    all_to_all x2, waiting for transfers between devices, exchanged(): return lax.all_to_all(x, axis, split_axis=0, concat_axis=0, tiled=True)  14.3 us
    all_to_all x1, blocking collectives, mirrored(): lax.all_to_all(x, ('kv_1', 'tp'), split_axis=0, concat_axis=0, tiled=True...  11.4 us
    ppermute x3, starting transfers between devices, layer(): lax.ppermute(w_own, 'kv_1', [(i, (i + step) % Y) for i in range(Y)])  8.37 us
    ppermute x3, waiting for transfers between devices, layer(): lax.ppermute(w_own, 'kv_1', [(i, (i + step) % Y) for i in range(Y)])  6.14 us
    ppermute x3, starting transfers between devices, swapped(): return lax.ppermute(x, 'tp', [(0, 1), (1, 0)])  5.88 us
    ppermute x3, waiting for transfers between devices, swapped(): return lax.ppermute(x, 'tp', [(0, 1), (1, 0)])  3.6 us
  transfers between devices with their start and end apart: 8, of which 5 were waited for; matrix products, arithmetic and copies ran while one was open for 0% of the time, Pallas kernels for 2%

profile of v3, /device:TPU:6, one launch (start us, length us, event | category | flops | bytes accessed | tf_op | source)
XLA Modules:
  0.0 151.4 jit_solution(7729107635725644253)
XLA Ops:
  0.6 2.6 %shard_map.192 = bf16[4,32,3328]{2,1,0:T(8,128)(2,1)} custom-call(bf16[64,128]{1,0:T(8,128)(2,1)} %bitcast.39, f32[1,64]{1,0:T(1,128)} %bitcast.43, bf16[8,64]{1,0:T(8,128)(2,1)} %bitcast.41, bf16[8,64]{1,0:T(8,128)(2,1)} %bitcast.42, bf16[64,1024]{1,0:T(8,128)(2,1)} %wq_ref.1, bf16[64,1024]{1,0:T(8,128)(2,1)} %wk_ref.1, bf16[64,1024]{1,0:T(8,128)(2,1)} %wv_ref.1), custom_call_target="tpu_custom_call" | custom-call | flops 52428800 | bytes 1000000 | tf_op jit(solution)/shard_map/pallas_call | solution.py:294
  3.2 17.4 %all_to_all.35.in_ref = bf16[4,32,3328]{2,1,0:T(8,128)(2,1)S(1)} all-to-all(bf16[4,32,3328]{2,1,0:T(8,128)(2,1)} %shard_map.192), channel_id=1, replica_groups=mesh['dp'=4,'kv_0'=16,'kv_1'=4,'tp'=2] {'kv_1'}, dimensions={0} | all-to-all | bytes 1703936 | tf_op jit(solution)/shard_map/all_to_all | solution.py:24
  20.7 0.0 copy-start
  20.7 0.8 shard_map.193
  21.5 0.0 copy-start.4
  21.5 15.3 %all-to-all-start.1 = ((bf16[16,2,3200]{2,1,0:T(2,128)(2,1)}), bf16[16,2,3200]{2,1,0:T(2,128)(2,1)S(1)}, u32[]{:S(2)}, u32[]{:S(2)}) async-start(bf16[16,2,3200]{2,1,0:T(2,128)(2,1)} %get-tuple-element.13), calls=%async_computation.1 | async-start | bytes 409600 | tf_op jit(solution)/shard_map/all_to_all | solution.py:24
  36.8 0.0 copy-done.4
  36.8 3.1 %collective-permute-start.2 = (bf16[64,1024]{1,0:T(8,128)(2,1)S(1)}, bf16[64,1024]{1,0:T(8,128)(2,1)S(1)}, u32[]{:S(2)}, u32[]{:S(2)}) collective-permute-start(bf16[64,1024]{1,0:T(8,128)(2,1)S(1)} %bitcast.29), channel_id=1, source_target_pairs={{0,6},{2,0},{4,2},{6,4},{1,7},{3,1},{5,3},{7,5},{8,14},{10,8},{12,... | collective-permute-start | bytes 393224 | tf_op jit(solution)/shard_map/ppermute | solution.py:308
  39.9 3.4 %collective-permute-start.1 = (bf16[64,1024]{1,0:T(8,128)(2,1)S(1)}, bf16[64,1024]{1,0:T(8,128)(2,1)S(1)}, u32[]{:S(2)}, u32[]{:S(2)}) collective-permute-start(bf16[64,1024]{1,0:T(8,128)(2,1)S(1)} %bitcast.30), channel_id=1, source_target_pairs={{0,4},{2,6},{4,0},{6,2},{1,5},{3,7},{5,1},{7,3},{8,12},{10,14},{12... | collective-permute-start | bytes 393224 | tf_op jit(solution)/shard_map/ppermute | solution.py:308
  43.3 1.9 %collective-permute-start = (bf16[64,1024]{1,0:T(8,128)(2,1)S(1)}, bf16[64,1024]{1,0:T(8,128)(2,1)S(1)}, u32[]{:S(2)}, u32[]{:S(2)}) collective-permute-start(bf16[64,1024]{1,0:T(8,128)(2,1)S(1)} %bitcast.31), channel_id=1, source_target_pairs={{0,2},{2,4},{4,6},{6,0},{1,3},{3,5},{5,7},{7,1},{8,10},{10,12},{12... | collective-permute-start | bytes 393224 | tf_op jit(solution)/shard_map/ppermute | solution.py:308
  45.2 0.0 collective-permute-done.2.w3_ref
  45.2 4.4 %collective-permute-done.1.w2_ref = bf16[64,1024]{1,0:T(8,128)(2,1)S(1)} collective-permute-done((bf16[64,1024]{1,0:T(8,128)(2,1)S(1)}, bf16[64,1024]{1,0:T(8,128)(2,1)S(1)}, u32[]{:S(2)}, u32[]{:S(2)}) %collective-permute-start.1) | collective-permute-done | bytes 131104 | tf_op jit(solution)/shard_map/ppermute | solution.py:308
  49.7 1.7 %collective-permute-done.w1_ref = bf16[64,1024]{1,0:T(8,128)(2,1)S(1)} collective-permute-done((bf16[64,1024]{1,0:T(8,128)(2,1)S(1)}, bf16[64,1024]{1,0:T(8,128)(2,1)S(1)}, u32[]{:S(2)}, u32[]{:S(2)}) %collective-permute-start) | collective-permute-done | bytes 131104 | tf_op jit(solution)/shard_map/ppermute | solution.py:308
  51.4 0.0 copy-start.7
  51.4 0.0 copy-start.8
  51.4 0.1 pad_maximum_fusion
  51.5 0.0 copy-start.5
  51.5 1.9 %collective-permute-start.3 = (bf16[4,64,1024]{2,1,0:T(8,128)(2,1)S(1)}, bf16[4,64,1024]{2,1,0:T(8,128)(2,1)S(1)}, u32[]{:S(2)}, u32[]{:S(2)}) collective-permute-start(bf16[4,64,1024]{2,1,0:T(8,128)(2,1)S(1)} %pad_maximum_fusion), channel_id=1, source_target_pairs={{0,1},{1,0},{2,3},{3,2},{4,5},{5,4},{6,7},{7,6},{8,9},{9,8},{10,11... | collective-permute-start | bytes 1572872 | tf_op jit(solution)/shard_map/ppermute | solution.py:35
  53.4 0.0 copy-done.7
  53.4 0.0 copy-done.8
  53.4 0.0 copy-done.9
  53.4 0.0 all-to-all-done.1.in_ref
  53.4 0.0 copy-done
  53.5 0.0 copy-done.5
  53.5 2.6 %shard_map.194 = (bf16[32,8,128]{2,1,0:T(8,128)(2,1)}, f32[16,128,128]{2,1,0:T(8,128)}, f32[16,128]{1,0:T(8,128)}, f32[2,8]{1,0:T(2,128)}) custom-call(bf16[16,2,3200]{2,1,0:T(2,128)(2,1)S(1)} %all-to-all-done.1.in_ref, f32[4,8]{1,0:T(4,128)S(1)} %pad_maximum_fusion.1.small_ref, f32[16,128,128]{2,1,0:T(8,128)S(1)} %bitcast.25, f32[16,128]{1,0:T(8,128)S(1)} %bitcast.37), custom_call_target="tpu_custom_call" | custom-call | flops 10000000 | bytes 1000000 | tf_op jit(solution)/shard_map/pallas_call | solution.py:313
  56.1 12.4 %all-to-all-start.2 = ((bf16[32,8,128]{2,1,0:T(8,128)(2,1)}), bf16[32,8,128]{2,1,0:T(8,128)(2,1)S(1)}, u32[]{:S(2)}, u32[]{:S(2)}) async-start(bf16[32,8,128]{2,1,0:T(8,128)(2,1)} %get-tuple-element.14), calls=%async_computation.2 | async-start | bytes 131072 | tf_op jit(solution)/shard_map/all_to_all | solution.py:24
  68.5 0.1 pad_add_fusion.place_ref
  68.6 14.3 %all-to-all-done.2 = bf16[32,8,128]{2,1,0:T(8,128)(2,1)S(1)} async-done(((bf16[32,8,128]{2,1,0:T(8,128)(2,1)}), bf16[32,8,128]{2,1,0:T(8,128)(2,1)S(1)}, u32[]{:S(2)}, u32[]{:S(2)}) %all-to-all-start.2) | async-done | bytes 65568 | tf_op jit(solution)/shard_map/all_to_all | solution.py:24
  82.9 0.0 collective-permute-done.3.other_ref
  82.9 0.0 copy-start.3
  83.0 1.0 shard_map.195
  84.0 16.7 %all_to_all.36 = bf16[16,16,256]{2,1,0:T(8,128)(2,1)S(1)} all-to-all(bf16[16,16,256]{2,1,0:T(8,128)(2,1)S(1)} %shard_map.195), channel_id=1, replica_groups=mesh['dp'=4,'kv_0'=16,'kv_1'=4,'tp'=2] {'kv_0'}, dimensions={0} | all-to-all | bytes 262144 | tf_op jit(solution)/shard_map/all_to_all | solution.py:24
  100.7 0.0 copy-start.6
  100.7 10.6 %all_to_all.37.own_ref = bf16[4,256,256]{2,1,0:T(8,128)(2,1)S(1)} all-to-all(bf16[4,256,256]{2,1,0:T(8,128)(2,1)S(1)} %shard_map.196), channel_id=1, replica_groups=mesh['dp'=4,'kv_0'=16,'kv_1'=4,'tp'=2] {'kv_1'}, dimensions={0} | all-to-all | bytes 1048576 | tf_op jit(solution)/shard_map/all_to_all | solution.py:24
  111.3 1.9 %collective-permute-start.4 = (bf16[4,256,256]{2,1,0:T(8,128)(2,1)S(1)}, bf16[4,256,256]{2,1,0:T(8,128)(2,1)S(1)}, u32[]{:S(2)}, u32[]{:S(2)}) collective-permute-start(bf16[4,256,256]{2,1,0:T(8,128)(2,1)S(1)} %all_to_all.37.own_ref), channel_id=1, source_target_pairs={{0,1},{1,0},{2,3},{3,2},{4,5},{5,4},{6,7},{7,6},{8,9},{9,8},{10,11... | collective-permute-start | bytes 1572872 | tf_op jit(solution)/shard_map/ppermute | solution.py:35
  113.3 0.0 copy-done.6
  113.3 1.9 %collective-permute-done.4.other_ref = bf16[4,256,256]{2,1,0:T(8,128)(2,1)S(1)} collective-permute-done((bf16[4,256,256]{2,1,0:T(8,128)(2,1)S(1)}, bf16[4,256,256]{2,1,0:T(8,128)(2,1)S(1)}, u32[]{:S(2)}, u32[]{:S(2)}) %collective-permute-start.4) | collective-permute-done | bytes 524320 | tf_op jit(solution)/shard_map/ppermute | solution.py:35
  115.1 0.0 copy-done.3
  115.1 0.0 copy-done.1
  115.1 0.0 copy-done.2
  115.2 1.9 %shard_map.197 = (f32[4,512,128]{2,1,0:T(8,128)S(1)}, bf16[4,512,128]{2,1,0:T(8,128)(2,1)S(1)}, bf16[32,128]{1,0:T(8,128)(2,1)S(1)}) custom-call(s32[4]{0:T(128)S(1)} %pad_add_fusion.place_ref, bf16[4,256,256]{2,1,0:T(8,128)(2,1)S(1)} %all_to_all.37.own_ref, bf16[4,256,256]{2,1,0:T(8,128)(2,1)S(1)} %collective-permute-done.4.other_ref, ...), custom_call_target="tpu_custom_call" | custom-call | flops 276824064 | bytes 1000000 | tf_op jit(solution)/shard_map/pallas_call | solution.py:338
  117.0 2.1 %collective-permute-start.5 = (bf16[4,512,128]{2,1,0:T(8,128)(2,1)S(1)}, bf16[4,512,128]{2,1,0:T(8,128)(2,1)S(1)}, u32[]{:S(2)}, u32[]{:S(2)}) collective-permute-start(bf16[4,512,128]{2,1,0:T(8,128)(2,1)S(1)} %get-tuple-element.17), channel_id=1, source_target_pairs={{0,1},{1,0},{2,3},{3,2},{4,5},{5,4},{6,7},{7,6},{8,9},{9,8},{10,11... | collective-permute-start | bytes 1572872 | tf_op jit(solution)/shard_map/ppermute | solution.py:35
  119.1 1.7 %collective-permute-done.5 = bf16[4,512,128]{2,1,0:T(8,128)(2,1)S(1)} collective-permute-done((bf16[4,512,128]{2,1,0:T(8,128)(2,1)S(1)}, bf16[4,512,128]{2,1,0:T(8,128)(2,1)S(1)}, u32[]{:S(2)}, u32[]{:S(2)}) %collective-permute-start.5) | collective-permute-done | bytes 524320 | tf_op jit(solution)/shard_map/ppermute | solution.py:35
  120.8 0.1 add_convert_fusion
  121.0 11.4 %all_to_all.38 = bf16[4,512,128]{2,1,0:T(8,128)(2,1)S(1)} all-to-all(bf16[4,512,128]{2,1,0:T(8,128)(2,1)S(1)} %add_convert_fusion), channel_id=1, replica_groups={{0,2,4,6},{5,7,1,3},{8,10,12,14},{13,15,9,11},{16,18,20,22},{21,23,17,1..., dimensions={0} | all-to-all | bytes 1048576 | tf_op jit(solution)/shard_map/all_to_all | solution.py:29
  132.4 0.1 reduce_sum.12
  132.5 18.2 %all_to_all.39.in_ref = bf16[16,32,128]{2,1,0:T(8,128)(2,1)S(1)} all-to-all(bf16[16,32,128]{2,1,0:T(8,128)(2,1)S(1)} %bitcast.38), channel_id=1, replica_groups=mesh['dp'=4,'kv_0'=16,'kv_1'=4,'tp'=2] {'kv_0'}, dimensions={0} | all-to-all | bytes 262144 | tf_op jit(solution)/shard_map/all_to_all | solution.py:24
  150.6 0.8 shard_map.198
  (7 shorter events, 0.1 us)
Async XLA Ops:
  20.7 32.8 %copy-start = (f32[2,8,128,128]{3,2,1,0:T(8,128)S(1)}, f32[2,8,128,128]{3,2,1,0:T(8,128)}, u32[]{:S(2)}) copy-start(f32[2,8,128,128]{3,2,1,0:T(8,128)} %param.26) | copy-start | bytes 3145732
  21.5 15.3 %copy-start.4 = (bf16[1024,64]{0,1:T(8,128)(2,1)S(1)}, bf16[1024,64]{0,1:T(8,128)(2,1)}, u32[]{:S(2)}) copy-start(bf16[1024,64]{0,1:T(8,128)(2,1)} %param.29) | copy-start | bytes 393220
  21.5 32.0 %all-to-all-start.1 = ((bf16[16,2,3200]{2,1,0:T(2,128)(2,1)}), bf16[16,2,3200]{2,1,0:T(2,128)(2,1)S(1)}, u32[]{:S(2)}, u32[]{:S(2)}) async-start(bf16[16,2,3200]{2,1,0:T(2,128)(2,1)} %get-tuple-element.13), calls=%async_computation.1 | async-start | bytes 409600 | tf_op jit(solution)/shard_map/all_to_all | solution.py:24
  36.8 8.4 %collective-permute-start.2 = (bf16[64,1024]{1,0:T(8,128)(2,1)S(1)}, bf16[64,1024]{1,0:T(8,128)(2,1)S(1)}, u32[]{:S(2)}, u32[]{:S(2)}) collective-permute-start(bf16[64,1024]{1,0:T(8,128)(2,1)S(1)} %bitcast.29), channel_id=1, source_target_pairs={{0,6},{2,0},{4,2},{6,4},{1,7},{3,1},{5,3},{7,5},{8,14},{10,8},{12,... | collective-permute-start | bytes 393224 | tf_op jit(solution)/shard_map/ppermute | solution.py:308
  39.9 9.7 %collective-permute-start.1 = (bf16[64,1024]{1,0:T(8,128)(2,1)S(1)}, bf16[64,1024]{1,0:T(8,128)(2,1)S(1)}, u32[]{:S(2)}, u32[]{:S(2)}) collective-permute-start(bf16[64,1024]{1,0:T(8,128)(2,1)S(1)} %bitcast.30), channel_id=1, source_target_pairs={{0,4},{2,6},{4,0},{6,2},{1,5},{3,7},{5,1},{7,3},{8,12},{10,14},{12... | collective-permute-start | bytes 393224 | tf_op jit(solution)/shard_map/ppermute | solution.py:308
  43.3 8.1 %collective-permute-start = (bf16[64,1024]{1,0:T(8,128)(2,1)S(1)}, bf16[64,1024]{1,0:T(8,128)(2,1)S(1)}, u32[]{:S(2)}, u32[]{:S(2)}) collective-permute-start(bf16[64,1024]{1,0:T(8,128)(2,1)S(1)} %bitcast.31), channel_id=1, source_target_pairs={{0,2},{2,4},{4,6},{6,0},{1,3},{3,5},{5,7},{7,1},{8,10},{10,12},{12... | collective-permute-start | bytes 393224 | tf_op jit(solution)/shard_map/ppermute | solution.py:308
  51.4 2.0 %copy-start.7 = (f32[2,8]{1,0:T(2,128)S(1)}, f32[2,8]{1,0:T(2,128)}, u32[]{:S(2)}) copy-start(f32[2,8]{1,0:T(2,128)} %param.28) | copy-start | bytes 196
  51.4 2.0 %copy-start.8 = (f32[8]{0:T(128)S(1)}, f32[8]{0:T(128)}, u32[]{:S(2)}) copy-start(f32[8]{0:T(128)} %param.25) | copy-start | bytes 100
  51.4 2.0 %copy-start.9 = (f32[8]{0:T(128)S(1)}, f32[8]{0:T(128)}, u32[]{:S(2)}) copy-start(f32[8]{0:T(128)} %param.24) | copy-start | bytes 100
  51.5 2.0 %copy-start.5 = (f32[2,8,128]{2,1,0:T(8,128)S(1)}, f32[2,8,128]{2,1,0:T(8,128)}, u32[]{:S(2)}) copy-start(f32[2,8,128]{2,1,0:T(8,128)} %param.27) | copy-start | bytes 24580
  51.5 31.5 %collective-permute-start.3 = (bf16[4,64,1024]{2,1,0:T(8,128)(2,1)S(1)}, bf16[4,64,1024]{2,1,0:T(8,128)(2,1)S(1)}, u32[]{:S(2)}, u32[]{:S(2)}) collective-permute-start(bf16[4,64,1024]{2,1,0:T(8,128)(2,1)S(1)} %pad_maximum_fusion), channel_id=1, source_target_pairs={{0,1},{1,0},{2,3},{3,2},{4,5},{5,4},{6,7},{7,6},{8,9},{9,8},{10,11... | collective-permute-start | bytes 1572872 | tf_op jit(solution)/shard_map/ppermute | solution.py:35
  56.1 26.8 %all-to-all-start.2 = ((bf16[32,8,128]{2,1,0:T(8,128)(2,1)}), bf16[32,8,128]{2,1,0:T(8,128)(2,1)S(1)}, u32[]{:S(2)}, u32[]{:S(2)}) async-start(bf16[32,8,128]{2,1,0:T(8,128)(2,1)} %get-tuple-element.14), calls=%async_computation.2 | async-start | bytes 131072 | tf_op jit(solution)/shard_map/all_to_all | solution.py:24
  82.9 32.2 %copy-start.3 = (bf16[88,4096]{1,0:T(8,128)(2,1)S(1)}, bf16[88,4096]{1,0:T(8,128)(2,1)}, u32[]{:S(2)}) copy-start(bf16[88,4096]{1,0:T(8,128)(2,1)} %wd_ref.1) | copy-start | bytes 2162692
  100.7 14.5 %copy-start.1 = (bf16[4096,88]{0,1:T(8,128)(2,1)S(1)}, bf16[4096,88]{0,1:T(8,128)(2,1)}, u32[]{:S(2)}) copy-start(bf16[4096,88]{0,1:T(8,128)(2,1)} %param.31) | copy-start | bytes 2162692
  100.7 14.5 %copy-start.2 = (bf16[4096,88]{0,1:T(8,128)(2,1)S(1)}, bf16[4096,88]{0,1:T(8,128)(2,1)}, u32[]{:S(2)}) copy-start(bf16[4096,88]{0,1:T(8,128)(2,1)} %param.32) | copy-start | bytes 2162692
  100.7 12.5 %copy-start.6 = (f32[4096]{0:T(1024)S(1)}, f32[4096]{0:T(1024)}, u32[]{:S(2)}) copy-start(f32[4096]{0:T(1024)} %param.30) | copy-start | bytes 49156
  111.3 3.8 %collective-permute-start.4 = (bf16[4,256,256]{2,1,0:T(8,128)(2,1)S(1)}, bf16[4,256,256]{2,1,0:T(8,128)(2,1)S(1)}, u32[]{:S(2)}, u32[]{:S(2)}) collective-permute-start(bf16[4,256,256]{2,1,0:T(8,128)(2,1)S(1)} %all_to_all.37.own_ref), channel_id=1, source_target_pairs={{0,1},{1,0},{2,3},{3,2},{4,5},{5,4},{6,7},{7,6},{8,9},{9,8},{10,11... | collective-permute-start | bytes 1572872 | tf_op jit(solution)/shard_map/ppermute | solution.py:35
  117.0 3.8 %collective-permute-start.5 = (bf16[4,512,128]{2,1,0:T(8,128)(2,1)S(1)}, bf16[4,512,128]{2,1,0:T(8,128)(2,1)S(1)}, u32[]{:S(2)}, u32[]{:S(2)}) collective-permute-start(bf16[4,512,128]{2,1,0:T(8,128)(2,1)S(1)} %get-tuple-element.17), channel_id=1, source_target_pairs={{0,1},{1,0},{2,3},{3,2},{4,5},{5,4},{6,7},{7,6},{8,9},{9,8},{10,11... | collective-permute-start | bytes 1572872 | tf_op jit(solution)/shard_map/ppermute | solution.py:35

commit v4 on v3

--- a/solution.py
+++ b/solution.py
@@ -241,7 +241,7 @@
             y = 2 * (m % 2) + pair
             lower = part[64 * pair : 64 * pair + HALF]
             upper = part[64 * pair + HALF : 64 * pair + 64]
-            keep_ref[mine[y], HALF * z : HALF * (z + 1), :] = jnp.where(first, lower, upper)
+            keep_ref[mine[y], HALF * z : HALF * (z + 1), :] = jnp.where(first, lower, upper).astype(bf16)
             send_ref[theirs[y], HALF * z : HALF * (z + 1), :] = jnp.where(first, upper, lower).astype(bf16)
 
 
@@ -338,7 +338,7 @@
     keep, send, residual = called(
         mlp_kernel,
         (
-            shape((Y, BLOCK, ROWS), f32),
+            shape((Y, BLOCK, ROWS), bf16),
             shape((Y, BLOCK, ROWS), bf16),
             shape((HALF, ROWS), bf16),
         ),
@@ -346,7 +346,7 @@
         in_specs=[IN_SMEM] + [IN_VMEM] * 6,
         scratch_shapes=[pltpu.VMEM((ROWS, D), bf16), pltpu.VMEM((ROWS, 256), bf16)],
     )(place, spread, other, gain_mlp.reshape(Z, 256), w_gate.T, w_up.T, w_down)
-    terms = (keep + swapped(send).astype(f32)).astype(bf16)
+    terms = (keep.astype(f32) + swapped(send).astype(f32)).astype(bf16)
     terms = mirrored(terms).astype(f32).sum(axis=0).astype(bf16)
     terms = exchanged(terms.reshape(Z, HALF, ROWS), "kv_0")
     mixed = called(finish_kernel, shape((HALF, ROWS), bf16), flops=10**6)(terms, residual)

time: 152 us -> 152 us (level)
  no operation moved by 1% of the time
where the time goes in v4:
time: 152 us; the launch traced here: 151 us
  blocking collectives  74.3 us (49%)
  starting transfers between devices  42 us (28%)
  waiting for transfers between devices  24 us (16%)
  Pallas kernels  9.72 us (6%)
    all_to_all x4, blocking collectives, exchanged(): return lax.all_to_all(x, axis, split_axis=0, concat_axis=0, tiled=True)  62.9 us
    all_to_all x2, starting transfers between devices, exchanged(): return lax.all_to_all(x, axis, split_axis=0, concat_axis=0, tiled=True)  27.7 us
    all_to_all x2, waiting for transfers between devices, exchanged(): return lax.all_to_all(x, axis, split_axis=0, concat_axis=0, tiled=True)  14.3 us
    all_to_all x1, blocking collectives, mirrored(): lax.all_to_all(x, ('kv_1', 'tp'), split_axis=0, concat_axis=0, tiled=True...  11.4 us
    ppermute x3, starting transfers between devices, layer(): lax.ppermute(w_own, 'kv_1', [(i, (i + step) % Y) for i in range(Y)])  8.37 us
    ppermute x3, waiting for transfers between devices, layer(): lax.ppermute(w_own, 'kv_1', [(i, (i + step) % Y) for i in range(Y)])  6.14 us
    ppermute x3, starting transfers between devices, swapped(): return lax.ppermute(x, 'tp', [(0, 1), (1, 0)])  5.88 us
    ppermute x3, waiting for transfers between devices, swapped(): return lax.ppermute(x, 'tp', [(0, 1), (1, 0)])  3.6 us
  transfers between devices with their start and end apart: 8, of which 5 were waited for; matrix products, arithmetic and copies ran while one was open for 0% of the time, Pallas kernels for 2%

profile of v4, /device:TPU:6, one launch (start us, length us, event | category | flops | bytes accessed | tf_op | source)
XLA Modules:
  0.0 151.4 jit_solution(2426148105205021560)
XLA Ops:
  0.6 2.6 %shard_map.192 = bf16[4,32,3328]{2,1,0:T(8,128)(2,1)} custom-call(bf16[64,128]{1,0:T(8,128)(2,1)} %bitcast.39, f32[1,64]{1,0:T(1,128)} %bitcast.43, bf16[8,64]{1,0:T(8,128)(2,1)} %bitcast.41, bf16[8,64]{1,0:T(8,128)(2,1)} %bitcast.42, bf16[64,1024]{1,0:T(8,128)(2,1)} %wq_ref.1, bf16[64,1024]{1,0:T(8,128)(2,1)} %wk_ref.1, bf16[64,1024]{1,0:T(8,128)(2,1)} %wv_ref.1), custom_call_target="tpu_custom_call" | custom-call | flops 52428800 | bytes 1000000 | tf_op jit(solution)/shard_map/pallas_call | solution.py:294
  3.2 17.4 %all_to_all.35.in_ref = bf16[4,32,3328]{2,1,0:T(8,128)(2,1)S(1)} all-to-all(bf16[4,32,3328]{2,1,0:T(8,128)(2,1)} %shard_map.192), channel_id=1, replica_groups=mesh['dp'=4,'kv_0'=16,'kv_1'=4,'tp'=2] {'kv_1'}, dimensions={0} | all-to-all | bytes 1703936 | tf_op jit(solution)/shard_map/all_to_all | solution.py:24
  20.7 0.0 copy-start
  20.7 0.8 shard_map.193
  21.5 0.0 copy-start.4
  21.5 15.3 %all-to-all-start.1 = ((bf16[16,2,3200]{2,1,0:T(2,128)(2,1)}), bf16[16,2,3200]{2,1,0:T(2,128)(2,1)S(1)}, u32[]{:S(2)}, u32[]{:S(2)}) async-start(bf16[16,2,3200]{2,1,0:T(2,128)(2,1)} %get-tuple-element.13), calls=%async_computation.1 | async-start | bytes 409600 | tf_op jit(solution)/shard_map/all_to_all | solution.py:24
  36.8 0.0 copy-done.4
  36.8 3.1 %collective-permute-start.2 = (bf16[64,1024]{1,0:T(8,128)(2,1)S(1)}, bf16[64,1024]{1,0:T(8,128)(2,1)S(1)}, u32[]{:S(2)}, u32[]{:S(2)}) collective-permute-start(bf16[64,1024]{1,0:T(8,128)(2,1)S(1)} %bitcast.29), channel_id=1, source_target_pairs={{0,6},{2,0},{4,2},{6,4},{1,7},{3,1},{5,3},{7,5},{8,14},{10,8},{12,... | collective-permute-start | bytes 393224 | tf_op jit(solution)/shard_map/ppermute | solution.py:308
  39.9 3.4 %collective-permute-start.1 = (bf16[64,1024]{1,0:T(8,128)(2,1)S(1)}, bf16[64,1024]{1,0:T(8,128)(2,1)S(1)}, u32[]{:S(2)}, u32[]{:S(2)}) collective-permute-start(bf16[64,1024]{1,0:T(8,128)(2,1)S(1)} %bitcast.30), channel_id=1, source_target_pairs={{0,4},{2,6},{4,0},{6,2},{1,5},{3,7},{5,1},{7,3},{8,12},{10,14},{12... | collective-permute-start | bytes 393224 | tf_op jit(solution)/shard_map/ppermute | solution.py:308
  43.3 1.9 %collective-permute-start = (bf16[64,1024]{1,0:T(8,128)(2,1)S(1)}, bf16[64,1024]{1,0:T(8,128)(2,1)S(1)}, u32[]{:S(2)}, u32[]{:S(2)}) collective-permute-start(bf16[64,1024]{1,0:T(8,128)(2,1)S(1)} %bitcast.31), channel_id=1, source_target_pairs={{0,2},{2,4},{4,6},{6,0},{1,3},{3,5},{5,7},{7,1},{8,10},{10,12},{12... | collective-permute-start | bytes 393224 | tf_op jit(solution)/shard_map/ppermute | solution.py:308
  45.2 0.0 collective-permute-done.2.w3_ref
  45.2 4.4 %collective-permute-done.1.w2_ref = bf16[64,1024]{1,0:T(8,128)(2,1)S(1)} collective-permute-done((bf16[64,1024]{1,0:T(8,128)(2,1)S(1)}, bf16[64,1024]{1,0:T(8,128)(2,1)S(1)}, u32[]{:S(2)}, u32[]{:S(2)}) %collective-permute-start.1) | collective-permute-done | bytes 131104 | tf_op jit(solution)/shard_map/ppermute | solution.py:308
  49.7 1.7 %collective-permute-done.w1_ref = bf16[64,1024]{1,0:T(8,128)(2,1)S(1)} collective-permute-done((bf16[64,1024]{1,0:T(8,128)(2,1)S(1)}, bf16[64,1024]{1,0:T(8,128)(2,1)S(1)}, u32[]{:S(2)}, u32[]{:S(2)}) %collective-permute-start) | collective-permute-done | bytes 131104 | tf_op jit(solution)/shard_map/ppermute | solution.py:308
  51.4 0.0 copy-start.7
  51.4 0.0 copy-start.8
  51.4 0.1 pad_maximum_fusion
  51.5 0.0 copy-start.5
  51.5 1.9 %collective-permute-start.3 = (bf16[4,64,1024]{2,1,0:T(8,128)(2,1)S(1)}, bf16[4,64,1024]{2,1,0:T(8,128)(2,1)S(1)}, u32[]{:S(2)}, u32[]{:S(2)}) collective-permute-start(bf16[4,64,1024]{2,1,0:T(8,128)(2,1)S(1)} %pad_maximum_fusion), channel_id=1, source_target_pairs={{0,1},{1,0},{2,3},{3,2},{4,5},{5,4},{6,7},{7,6},{8,9},{9,8},{10,11... | collective-permute-start | bytes 1572872 | tf_op jit(solution)/shard_map/ppermute | solution.py:35
  53.4 0.0 copy-done.7
  53.4 0.0 copy-done.8
  53.4 0.0 copy-done.9
  53.4 0.0 all-to-all-done.1.in_ref
  53.4 0.0 copy-done
  53.5 0.0 copy-done.5
  53.5 2.6 %shard_map.194 = (bf16[32,8,128]{2,1,0:T(8,128)(2,1)}, f32[16,128,128]{2,1,0:T(8,128)}, f32[16,128]{1,0:T(8,128)}, f32[2,8]{1,0:T(2,128)}) custom-call(bf16[16,2,3200]{2,1,0:T(2,128)(2,1)S(1)} %all-to-all-done.1.in_ref, f32[4,8]{1,0:T(4,128)S(1)} %pad_maximum_fusion.1.small_ref, f32[16,128,128]{2,1,0:T(8,128)S(1)} %bitcast.25, f32[16,128]{1,0:T(8,128)S(1)} %bitcast.37), custom_call_target="tpu_custom_call" | custom-call | flops 10000000 | bytes 1000000 | tf_op jit(solution)/shard_map/pallas_call | solution.py:313
  56.1 12.4 %all-to-all-start.2 = ((bf16[32,8,128]{2,1,0:T(8,128)(2,1)}), bf16[32,8,128]{2,1,0:T(8,128)(2,1)S(1)}, u32[]{:S(2)}, u32[]{:S(2)}) async-start(bf16[32,8,128]{2,1,0:T(8,128)(2,1)} %get-tuple-element.14), calls=%async_computation.2 | async-start | bytes 131072 | tf_op jit(solution)/shard_map/all_to_all | solution.py:24
  68.5 0.1 pad_add_fusion.place_ref
  68.6 14.3 %all-to-all-done.2 = bf16[32,8,128]{2,1,0:T(8,128)(2,1)S(1)} async-done(((bf16[32,8,128]{2,1,0:T(8,128)(2,1)}), bf16[32,8,128]{2,1,0:T(8,128)(2,1)S(1)}, u32[]{:S(2)}, u32[]{:S(2)}) %all-to-all-start.2) | async-done | bytes 65568 | tf_op jit(solution)/shard_map/all_to_all | solution.py:24
  82.9 0.0 collective-permute-done.3.other_ref
  82.9 0.0 copy-start.3
  83.0 1.0 shard_map.195
  84.0 16.7 %all_to_all.36 = bf16[16,16,256]{2,1,0:T(8,128)(2,1)S(1)} all-to-all(bf16[16,16,256]{2,1,0:T(8,128)(2,1)S(1)} %shard_map.195), channel_id=1, replica_groups=mesh['dp'=4,'kv_0'=16,'kv_1'=4,'tp'=2] {'kv_0'}, dimensions={0} | all-to-all | bytes 262144 | tf_op jit(solution)/shard_map/all_to_all | solution.py:24
  100.7 0.0 copy-start.6
  100.7 10.6 %all_to_all.37.own_ref = bf16[4,256,256]{2,1,0:T(8,128)(2,1)S(1)} all-to-all(bf16[4,256,256]{2,1,0:T(8,128)(2,1)S(1)} %shard_map.196), channel_id=1, replica_groups=mesh['dp'=4,'kv_0'=16,'kv_1'=4,'tp'=2] {'kv_1'}, dimensions={0} | all-to-all | bytes 1048576 | tf_op jit(solution)/shard_map/all_to_all | solution.py:24
  111.3 1.9 %collective-permute-start.4 = (bf16[4,256,256]{2,1,0:T(8,128)(2,1)S(1)}, bf16[4,256,256]{2,1,0:T(8,128)(2,1)S(1)}, u32[]{:S(2)}, u32[]{:S(2)}) collective-permute-start(bf16[4,256,256]{2,1,0:T(8,128)(2,1)S(1)} %all_to_all.37.own_ref), channel_id=1, source_target_pairs={{0,1},{1,0},{2,3},{3,2},{4,5},{5,4},{6,7},{7,6},{8,9},{9,8},{10,11... | collective-permute-start | bytes 1572872 | tf_op jit(solution)/shard_map/ppermute | solution.py:35
  113.3 0.0 copy-done.6
  113.3 1.9 %collective-permute-done.4.other_ref = bf16[4,256,256]{2,1,0:T(8,128)(2,1)S(1)} collective-permute-done((bf16[4,256,256]{2,1,0:T(8,128)(2,1)S(1)}, bf16[4,256,256]{2,1,0:T(8,128)(2,1)S(1)}, u32[]{:S(2)}, u32[]{:S(2)}) %collective-permute-start.4) | collective-permute-done | bytes 524320 | tf_op jit(solution)/shard_map/ppermute | solution.py:35
  115.1 0.0 copy-done.3
  115.1 0.0 copy-done.1
  115.1 0.0 copy-done.2
  115.2 1.9 %shard_map.197 = (bf16[4,512,128]{2,1,0:T(8,128)(2,1)S(1)}, bf16[4,512,128]{2,1,0:T(8,128)(2,1)S(1)}, bf16[32,128]{1,0:T(8,128)(2,1)S(1)}) custom-call(s32[4]{0:T(128)S(1)} %pad_add_fusion.place_ref, bf16[4,256,256]{2,1,0:T(8,128)(2,1)S(1)} %all_to_all.37.own_ref, bf16[4,256,256]{2,1,0:T(8,128)(2,1)S(1)} %collective-permute-done.4.other_ref, ...), custom_call_target="tpu_custom_call" | custom-call | flops 276824064 | bytes 1000000 | tf_op jit(solution)/shard_map/pallas_call | solution.py:338
  117.0 2.1 %collective-permute-start.5 = (bf16[4,512,128]{2,1,0:T(8,128)(2,1)S(1)}, bf16[4,512,128]{2,1,0:T(8,128)(2,1)S(1)}, u32[]{:S(2)}, u32[]{:S(2)}) collective-permute-start(bf16[4,512,128]{2,1,0:T(8,128)(2,1)S(1)} %get-tuple-element.17), channel_id=1, source_target_pairs={{0,1},{1,0},{2,3},{3,2},{4,5},{5,4},{6,7},{7,6},{8,9},{9,8},{10,11... | collective-permute-start | bytes 1572872 | tf_op jit(solution)/shard_map/ppermute | solution.py:35
  119.1 1.7 %collective-permute-done.5 = bf16[4,512,128]{2,1,0:T(8,128)(2,1)S(1)} collective-permute-done((bf16[4,512,128]{2,1,0:T(8,128)(2,1)S(1)}, bf16[4,512,128]{2,1,0:T(8,128)(2,1)S(1)}, u32[]{:S(2)}, u32[]{:S(2)}) %collective-permute-start.5) | collective-permute-done | bytes 524320 | tf_op jit(solution)/shard_map/ppermute | solution.py:35
  120.8 0.1 add_convert_fusion
  121.0 11.4 %all_to_all.38 = bf16[4,512,128]{2,1,0:T(8,128)(2,1)S(1)} all-to-all(bf16[4,512,128]{2,1,0:T(8,128)(2,1)S(1)} %add_convert_fusion), channel_id=1, replica_groups={{0,2,4,6},{5,7,1,3},{8,10,12,14},{13,15,9,11},{16,18,20,22},{21,23,17,1..., dimensions={0} | all-to-all | bytes 1048576 | tf_op jit(solution)/shard_map/all_to_all | solution.py:29
  132.4 0.1 reduce_sum.12
  132.5 18.2 %all_to_all.39.in_ref = bf16[16,32,128]{2,1,0:T(8,128)(2,1)S(1)} all-to-all(bf16[16,32,128]{2,1,0:T(8,128)(2,1)S(1)} %bitcast.38), channel_id=1, replica_groups=mesh['dp'=4,'kv_0'=16,'kv_1'=4,'tp'=2] {'kv_0'}, dimensions={0} | all-to-all | bytes 262144 | tf_op jit(solution)/shard_map/all_to_all | solution.py:24
  150.6 0.8 shard_map.198
  (7 shorter events, 0.1 us)
Async XLA Ops:
  20.7 32.8 %copy-start = (f32[2,8,128,128]{3,2,1,0:T(8,128)S(1)}, f32[2,8,128,128]{3,2,1,0:T(8,128)}, u32[]{:S(2)}) copy-start(f32[2,8,128,128]{3,2,1,0:T(8,128)} %param.26) | copy-start | bytes 3145732
  21.5 15.3 %copy-start.4 = (bf16[1024,64]{0,1:T(8,128)(2,1)S(1)}, bf16[1024,64]{0,1:T(8,128)(2,1)}, u32[]{:S(2)}) copy-start(bf16[1024,64]{0,1:T(8,128)(2,1)} %param.29) | copy-start | bytes 393220
  21.5 32.0 %all-to-all-start.1 = ((bf16[16,2,3200]{2,1,0:T(2,128)(2,1)}), bf16[16,2,3200]{2,1,0:T(2,128)(2,1)S(1)}, u32[]{:S(2)}, u32[]{:S(2)}) async-start(bf16[16,2,3200]{2,1,0:T(2,128)(2,1)} %get-tuple-element.13), calls=%async_computation.1 | async-start | bytes 409600 | tf_op jit(solution)/shard_map/all_to_all | solution.py:24
  36.8 8.4 %collective-permute-start.2 = (bf16[64,1024]{1,0:T(8,128)(2,1)S(1)}, bf16[64,1024]{1,0:T(8,128)(2,1)S(1)}, u32[]{:S(2)}, u32[]{:S(2)}) collective-permute-start(bf16[64,1024]{1,0:T(8,128)(2,1)S(1)} %bitcast.29), channel_id=1, source_target_pairs={{0,6},{2,0},{4,2},{6,4},{1,7},{3,1},{5,3},{7,5},{8,14},{10,8},{12,... | collective-permute-start | bytes 393224 | tf_op jit(solution)/shard_map/ppermute | solution.py:308
  39.9 9.7 %collective-permute-start.1 = (bf16[64,1024]{1,0:T(8,128)(2,1)S(1)}, bf16[64,1024]{1,0:T(8,128)(2,1)S(1)}, u32[]{:S(2)}, u32[]{:S(2)}) collective-permute-start(bf16[64,1024]{1,0:T(8,128)(2,1)S(1)} %bitcast.30), channel_id=1, source_target_pairs={{0,4},{2,6},{4,0},{6,2},{1,5},{3,7},{5,1},{7,3},{8,12},{10,14},{12... | collective-permute-start | bytes 393224 | tf_op jit(solution)/shard_map/ppermute | solution.py:308
  43.3 8.1 %collective-permute-start = (bf16[64,1024]{1,0:T(8,128)(2,1)S(1)}, bf16[64,1024]{1,0:T(8,128)(2,1)S(1)}, u32[]{:S(2)}, u32[]{:S(2)}) collective-permute-start(bf16[64,1024]{1,0:T(8,128)(2,1)S(1)} %bitcast.31), channel_id=1, source_target_pairs={{0,2},{2,4},{4,6},{6,0},{1,3},{3,5},{5,7},{7,1},{8,10},{10,12},{12... | collective-permute-start | bytes 393224 | tf_op jit(solution)/shard_map/ppermute | solution.py:308
  51.4 2.0 %copy-start.7 = (f32[2,8]{1,0:T(2,128)S(1)}, f32[2,8]{1,0:T(2,128)}, u32[]{:S(2)}) copy-start(f32[2,8]{1,0:T(2,128)} %param.28) | copy-start | bytes 196
  51.4 2.0 %copy-start.8 = (f32[8]{0:T(128)S(1)}, f32[8]{0:T(128)}, u32[]{:S(2)}) copy-start(f32[8]{0:T(128)} %param.25) | copy-start | bytes 100
  51.4 2.0 %copy-start.9 = (f32[8]{0:T(128)S(1)}, f32[8]{0:T(128)}, u32[]{:S(2)}) copy-start(f32[8]{0:T(128)} %param.24) | copy-start | bytes 100
  51.5 2.0 %copy-start.5 = (f32[2,8,128]{2,1,0:T(8,128)S(1)}, f32[2,8,128]{2,1,0:T(8,128)}, u32[]{:S(2)}) copy-start(f32[2,8,128]{2,1,0:T(8,128)} %param.27) | copy-start | bytes 24580
  51.5 31.5 %collective-permute-start.3 = (bf16[4,64,1024]{2,1,0:T(8,128)(2,1)S(1)}, bf16[4,64,1024]{2,1,0:T(8,128)(2,1)S(1)}, u32[]{:S(2)}, u32[]{:S(2)}) collective-permute-start(bf16[4,64,1024]{2,1,0:T(8,128)(2,1)S(1)} %pad_maximum_fusion), channel_id=1, source_target_pairs={{0,1},{1,0},{2,3},{3,2},{4,5},{5,4},{6,7},{7,6},{8,9},{9,8},{10,11... | collective-permute-start | bytes 1572872 | tf_op jit(solution)/shard_map/ppermute | solution.py:35
  56.1 26.8 %all-to-all-start.2 = ((bf16[32,8,128]{2,1,0:T(8,128)(2,1)}), bf16[32,8,128]{2,1,0:T(8,128)(2,1)S(1)}, u32[]{:S(2)}, u32[]{:S(2)}) async-start(bf16[32,8,128]{2,1,0:T(8,128)(2,1)} %get-tuple-element.14), calls=%async_computation.2 | async-start | bytes 131072 | tf_op jit(solution)/shard_map/all_to_all | solution.py:24
  82.9 32.2 %copy-start.3 = (bf16[88,4096]{1,0:T(8,128)(2,1)S(1)}, bf16[88,4096]{1,0:T(8,128)(2,1)}, u32[]{:S(2)}) copy-start(bf16[88,4096]{1,0:T(8,128)(2,1)} %wd_ref.1) | copy-start | bytes 2162692
  100.7 14.5 %copy-start.1 = (bf16[4096,88]{0,1:T(8,128)(2,1)S(1)}, bf16[4096,88]{0,1:T(8,128)(2,1)}, u32[]{:S(2)}) copy-start(bf16[4096,88]{0,1:T(8,128)(2,1)} %param.31) | copy-start | bytes 2162692
  100.7 14.5 %copy-start.2 = (bf16[4096,88]{0,1:T(8,128)(2,1)S(1)}, bf16[4096,88]{0,1:T(8,128)(2,1)}, u32[]{:S(2)}) copy-start(bf16[4096,88]{0,1:T(8,128)(2,1)} %param.32) | copy-start | bytes 2162692
  100.7 12.5 %copy-start.6 = (f32[4096]{0:T(1024)S(1)}, f32[4096]{0:T(1024)}, u32[]{:S(2)}) copy-start(f32[4096]{0:T(1024)} %param.30) | copy-start | bytes 49156
  111.3 3.8 %collective-permute-start.4 = (bf16[4,256,256]{2,1,0:T(8,128)(2,1)S(1)}, bf16[4,256,256]{2,1,0:T(8,128)(2,1)S(1)}, u32[]{:S(2)}, u32[]{:S(2)}) collective-permute-start(bf16[4,256,256]{2,1,0:T(8,128)(2,1)S(1)} %all_to_all.37.own_ref), channel_id=1, source_target_pairs={{0,1},{1,0},{2,3},{3,2},{4,5},{5,4},{6,7},{7,6},{8,9},{9,8},{10,11... | collective-permute-start | bytes 1572872 | tf_op jit(solution)/shard_map/ppermute | solution.py:35
  117.0 3.8 %collective-permute-start.5 = (bf16[4,512,128]{2,1,0:T(8,128)(2,1)S(1)}, bf16[4,512,128]{2,1,0:T(8,128)(2,1)S(1)}, u32[]{:S(2)}, u32[]{:S(2)}) collective-permute-start(bf16[4,512,128]{2,1,0:T(8,128)(2,1)S(1)} %get-tuple-element.17), channel_id=1, source_target_pairs={{0,1},{1,0},{2,3},{3,2},{4,5},{5,4},{6,7},{7,6},{8,9},{9,8},{10,11... | collective-permute-start | bytes 1572872 | tf_op jit(solution)/shard_map/ppermute | solution.py:35
